TPU v7x, 1024 devices: a whole 4x8x16 slice. The times are simulated.
1024 devices in a mesh: sp: 16 (over z), dp: 64 (over y, x, core).
Axes of the slice: x: 4, y: 8, z: 16, core: 2. Of those that a mesh axis runs over, the one named last changes fastest.
Arguments:
- queries: bfloat16 [64, 2048, 1024], P('dp', 'sp'), may hold values from -300 to 300
- keys: bfloat16 [64, 2048, 1024], P('dp', 'sp'), may hold values from -7 to 7
- values: bfloat16 [64, 2048, 1024], P('dp', 'sp'), may hold values from -6 to 6
- cum_gates: float32 [64, 16, 2048], P('dp', 'sp'), may hold values from -259 to 0, as said below
- out_weight: bfloat16 [1024, 2048], P(None, 'dp'), may hold values from -0.1875 to 0.1875
Outputs:
- mixed: bfloat16 [64, 2048, 2048], P('dp', 'sp')
Inputs may be any that keep to these rules, and one draw needn't show every extreme that they name: `cum_gates`: never rises along positions.
All inputs are finite; a program needn't handle non-finite values.
Results may differ from a plain program's by a relative error of at most 0.011.
Values may be sent and summed in bfloat16 or wider, within the bound.
No kernel may reach another device: no remote copies, remote signals or barrier semaphores. Data moves between devices by JAX's collectives and lax.ppermute only.
A program may use at most 64 MiB of HBM per device.

v0:
```python
import jax
import jax.numpy as jnp
from jax import lax
from jax.sharding import Mesh
from jax.sharding import PartitionSpec as P

DP = ("dp_0", "dp_1", "dp_2")


def in_order(blocks, dim):
    blocks = jnp.moveaxis(blocks, 0, dim)
    lengths = blocks.shape
    return blocks.reshape(*lengths[:dim], lengths[dim] * lengths[dim + 1], *lengths[dim + 2 :])


def gather_in_order(value, axes, order):
    blocks = value[None]
    for k in order:
        blocks = lax.all_gather(blocks, axes[k], axis=0, tiled=True)
    carried = [lax.axis_size(axes[k]) for k in reversed(order)]
    blocks = blocks.reshape(*carried, *value.shape)
    turned = sorted(range(len(order)), key=lambda place: order[len(order) - 1 - place])
    return blocks.transpose(*turned, *range(len(order), blocks.ndim)).reshape(-1, *value.shape)


def gather_axes(value, axes, order, dim):
    return in_order(gather_in_order(value, axes, order), dim)


def attend_heads(query_loc, key_loc, value_loc, cum_loc):
    length = query_loc.shape[0]
    head_count = cum_loc.shape[0]
    head_size = query_loc.shape[1] // head_count
    query_heads = query_loc.reshape(length, head_count, head_size).transpose(1, 0, 2)
    key_heads = key_loc.reshape(length, head_count, head_size).transpose(1, 0, 2)
    value_heads = value_loc.reshape(length, head_count, head_size).transpose(1, 0, 2)
    block_rows = min(512, length)
    block_count = length // block_rows
    query_blocks = query_heads.reshape(head_count, block_count, block_rows, head_size).transpose(
        1, 0, 2, 3
    )
    cum_blocks = cum_loc.reshape(head_count, block_count, block_rows).transpose(1, 0, 2)
    key_pos = jnp.arange(length)
    score_scale = head_size ** (-0.5)

    def one_block(packed):
        query_block, cum_block, block_index = packed
        scores = (
            jnp.einsum("hqd,hkd->hqk", query_block, key_heads, preferred_element_type=jnp.float32)
            * score_scale
        )
        scores = scores + cum_block[:, :, None] - cum_loc[:, None, :]
        query_pos = block_index * block_rows + jnp.arange(block_rows)
        scores = jnp.where(key_pos[None, :] <= query_pos[:, None], scores, -jnp.inf)
        row_max = jnp.max(scores, axis=-1, keepdims=True)
        expon = jnp.exp(scores - row_max)
        weights = (expon / jnp.sum(expon, axis=-1, keepdims=True)).astype(jnp.bfloat16)
        return jnp.einsum(
            "hqk,hkd->hqd", weights, value_heads, preferred_element_type=jnp.float32
        ).astype(jnp.bfloat16)

    results = lax.map(one_block, (query_blocks, cum_blocks, jnp.arange(block_count)))
    return results.transpose(0, 2, 1, 3).reshape(length, head_count * head_size)


def shards(queries, keys, values, cum_gates, out_weight):
    query_loc, key_loc, value_loc = (
        lax.all_to_all(queries[0], "sp", split_axis=1, concat_axis=0, tiled=True),
        lax.all_to_all(keys[0], "sp", split_axis=1, concat_axis=0, tiled=True),
        lax.all_to_all(values[0], "sp", split_axis=1, concat_axis=0, tiled=True),
    )
    head_out = attend_heads(query_loc, key_loc, value_loc, cum_gates[0])
    token_rows = lax.all_to_all(head_out, "sp", split_axis=0, concat_axis=1, tiled=True)
    mixed_rows = jnp.dot(
        token_rows, gather_axes(out_weight, DP, (1, 0, 2), 1), preferred_element_type=jnp.float32
    )
    return mixed_rows.astype(jnp.bfloat16)[None]


def solution(mesh):
    split = Mesh(mesh.devices.reshape(mesh.shape["sp"], 8, 4, 2), ("sp", "dp_0", "dp_1", "dp_2"))
    placed = (
        P(DP, "sp", None),
        P(DP, "sp", None),
        P(DP, "sp", None),
        P(DP, "sp", None),
        P(None, DP),
    )
    return jax.shard_map(
        shards, mesh=split, in_specs=placed, out_specs=P(DP, "sp", None), check_vma=False
    )
```

profile of v0, /device:TPU:56, one launch (start us, length us, event | category | flops | bytes accessed | tf_op | source)
XLA Modules:
  0.0 154.9 jit_solution(11761046255942086086)
XLA Ops:
  6.5 12.8 %all-gather = bf16[4096,32]{0,1:T(8,128)(2,1)S(1)} all-gather(bf16[1024,32]{0,1:T(8,128)(2,1)} %param.11), channel_id=2, replica_groups=mesh['sp'=16,'dp_0'=8,'dp_1'=4,'dp_2'=2] {'dp_1'}, dimensions={0}, use_global_device_ids=true | all-gather | bytes 327680 | tf_op jit(solution)/shard_map/all_gather | solution.py:19
  20.1 1.8 %copy.52 = bf16[1,128,1024]{1,2,0:T(8,128)(2,1)} copy(bf16[1,128,1024]{2,1,0:T(8,128)(2,1)} %param.7) | data formatting | bytes 524288 | tf_op args[0]
  21.9 18.9 %all-to-all-start = ((bf16[128,16,64]{0,2,1:T(8,128)(2,1)}), bf16[128,16,64]{0,2,1:T(8,128)(2,1)S(1)}, u32[]{:S(2)}, u32[]{:S(2)}) async-start(bf16[128,16,64]{0,2,1:T(8,128)(2,1)} %bitcast), calls=%async_computation | async-start | bytes 524288 | tf_op jit(solution)/shard_map/all_to_all | solution.py:68
  40.8 1.8 %copy.54 = bf16[1,128,1024]{1,2,0:T(8,128)(2,1)} copy(bf16[1,128,1024]{2,1,0:T(8,128)(2,1)} %param.8) | data formatting | bytes 524288 | tf_op args[1]
  42.5 14.5 %all-to-all-done = bf16[128,16,64]{0,2,1:T(8,128)(2,1)S(1)} async-done(((bf16[128,16,64]{0,2,1:T(8,128)(2,1)}), bf16[128,16,64]{0,2,1:T(8,128)(2,1)S(1)}, u32[]{:S(2)}, u32[]{:S(2)}) %all-to-all-start) | async-done | bytes 262176 | tf_op jit(solution)/shard_map/all_to_all | solution.py:68
  57.0 5.4 %all-to-all-start.1 = ((bf16[128,16,64]{0,2,1:T(8,128)(2,1)}), bf16[128,16,64]{0,2,1:T(8,128)(2,1)S(1)}, u32[]{:S(2)}, u32[]{:S(2)}) async-start(bf16[128,16,64]{0,2,1:T(8,128)(2,1)} %bitcast.3), calls=%async_computation.1 | async-start | bytes 524288 | tf_op jit(solution)/shard_map/all_to_all | solution.py:69
  62.5 1.8 %copy.56 = bf16[1,128,1024]{1,2,0:T(8,128)(2,1)} copy(bf16[1,128,1024]{2,1,0:T(8,128)(2,1)} %param.9) | data formatting | bytes 524288 | tf_op args[2]
  64.3 14.6 %all-to-all-done.1 = bf16[128,16,64]{0,2,1:T(8,128)(2,1)S(1)} async-done(((bf16[128,16,64]{0,2,1:T(8,128)(2,1)}), bf16[128,16,64]{0,2,1:T(8,128)(2,1)S(1)}, u32[]{:S(2)}, u32[]{:S(2)}) %all-to-all-start.1) | async-done | bytes 262176 | tf_op jit(solution)/shard_map/all_to_all | solution.py:69
  78.9 5.6 %all-to-all-start.2 = ((bf16[128,16,64]{0,2,1:T(8,128)(2,1)}), bf16[128,16,64]{0,2,1:T(8,128)(2,1)S(1)}, u32[]{:S(2)}, u32[]{:S(2)}) async-start(bf16[128,16,64]{0,2,1:T(8,128)(2,1)} %bitcast.7), calls=%async_computation.2 | async-start | bytes 524288 | tf_op jit(solution)/shard_map/all_to_all | solution.py:70
  85.1 16.6 %all-to-all-done.2 = bf16[128,16,64]{0,2,1:T(8,128)(2,1)S(1)} async-done(((bf16[128,16,64]{0,2,1:T(8,128)(2,1)}), bf16[128,16,64]{0,2,1:T(8,128)(2,1)S(1)}, u32[]{:S(2)}, u32[]{:S(2)}) %all-to-all-start.2) | async-done | bytes 262176 | tf_op jit(solution)/shard_map/all_to_all | solution.py:70
  102.0 17.3 %while.11 = (s32[]{:T(128)}, bf16[4,1,512,64]{2,3,1,0:T(8,128)(2,1)S(1)}, s32[4]{0:T(128)S(1)}, bf16[4,1,512,64]{3,2,1,0:T(8,128)(2,1)S(1)}, bf16[1,2048,64]{2,1...) while((s32[]{:T(128)}, ...), condition=%wide.region_3.4_spmd.clone, body=%wide.region_0.3_spmd.clone.sunk | while | flops 280002048 | bytes 13856917 | solution.py:62
  103.3 1.2 fusion.21
  105.3 1.1 fusion.23
  107.7 1.2 fusion.21
  109.6 1.1 fusion.23
  112.0 1.3 fusion.21
  113.9 1.1 fusion.23
  116.3 1.2 fusion.21
  118.3 1.1 fusion.23
  119.7 0.8 copy.62
  120.5 5.1 %all-to-all-start.3 = ((bf16[16,128,64]{1,2,0:T(8,128)(2,1)}), bf16[16,128,64]{1,2,0:T(8,128)(2,1)S(1)}, u32[]{:S(2)}, u32[]{:S(2)}) async-start(bf16[16,128,64]{1,2,0:T(8,128)(2,1)} %copy.62), calls=%async_computation.3 | async-start | bytes 524288 | tf_op jit(solution)/shard_map/all_to_all | solution.py:73
  125.6 5.0 %copy.64 = bf16[8,4,2,1024,32]{3,4,2,1,0:T(8,128)(2,1)} copy(bf16[8,4,2,1024,32]{3,4,1,0,2:T(8,128)(2,1)} %bitcast.66) | data formatting | bytes 8388608 | tf_op jit(solution)/shard_map/transpose | solution.py:23
  130.6 13.0 %all-to-all-done.3 = bf16[16,128,64]{1,2,0:T(8,128)(2,1)S(1)} async-done(((bf16[16,128,64]{1,2,0:T(8,128)(2,1)}), bf16[16,128,64]{1,2,0:T(8,128)(2,1)S(1)}, u32[]{:S(2)}, u32[]{:S(2)}) %all-to-all-start.3) | async-done | bytes 262176 | tf_op jit(solution)/shard_map/all_to_all | solution.py:73
  143.6 4.5 %fusion.12 = bf16[1,128,2048]{2,1,0:T(8,128)(2,1)} fusion(bf16[128,1024]{0,1:T(8,128)(2,1)S(1)} %bitcast.70, bf16[1024,2048]{0,1:T(8,128)(2,1)} %bitcast.65), kind=kOutput, calls=%fused_computation.18 | convolution fusion | flops 537133056 | bytes 4980736 | tf_op jit(solution)/shard_map/dot_general | solution.py:74
  (32 shorter events, 7.3 us)
Async XLA Ops:
  6.5 95.5 %all-gather.4.cloned.1.call-start = ((), (), s32[]{:S(2)}) async-start(), calls=%async_computation.4 | async-start | bytes 2359296 | tf_op jit(solution)/shard_map/all_gather | solution.py:19
  19.3 82.7 %copy-start = (f32[1,1,2048]{2,1,0:T(1,128)S(1)}, f32[1,1,2048]{2,1,0:T(1,128)}, u32[]{:S(2)}) copy-start(f32[1,1,2048]{2,1,0:T(1,128)} %param.10) | copy-start | bytes 24580
  21.9 35.1 %all-to-all-start = ((bf16[128,16,64]{0,2,1:T(8,128)(2,1)}), bf16[128,16,64]{0,2,1:T(8,128)(2,1)S(1)}, u32[]{:S(2)}, u32[]{:S(2)}) async-start(bf16[128,16,64]{0,2,1:T(8,128)(2,1)} %bitcast), calls=%async_computation | async-start | bytes 524288 | tf_op jit(solution)/shard_map/all_to_all | solution.py:68
  57.0 21.9 %all-to-all-start.1 = ((bf16[128,16,64]{0,2,1:T(8,128)(2,1)}), bf16[128,16,64]{0,2,1:T(8,128)(2,1)S(1)}, u32[]{:S(2)}, u32[]{:S(2)}) async-start(bf16[128,16,64]{0,2,1:T(8,128)(2,1)} %bitcast.3), calls=%async_computation.1 | async-start | bytes 524288 | tf_op jit(solution)/shard_map/all_to_all | solution.py:69
  78.9 22.8 %all-to-all-start.2 = ((bf16[128,16,64]{0,2,1:T(8,128)(2,1)}), bf16[128,16,64]{0,2,1:T(8,128)(2,1)S(1)}, u32[]{:S(2)}, u32[]{:S(2)}) async-start(bf16[128,16,64]{0,2,1:T(8,128)(2,1)} %bitcast.7), calls=%async_computation.2 | async-start | bytes 524288 | tf_op jit(solution)/shard_map/all_to_all | solution.py:70
  84.5 41.2 %all-gather.6.cloned.1.call-start = ((), (), s32[]{:S(2)}) async-start(), calls=%async_computation.5 | async-start | bytes 6291456 | tf_op jit(solution)/shard_map/all_gather | solution.py:19
  120.5 23.1 %all-to-all-start.3 = ((bf16[16,128,64]{1,2,0:T(8,128)(2,1)}), bf16[16,128,64]{1,2,0:T(8,128)(2,1)S(1)}, u32[]{:S(2)}, u32[]{:S(2)}) async-start(bf16[16,128,64]{1,2,0:T(8,128)(2,1)} %copy.62), calls=%async_computation.3 | async-start | bytes 524288 | tf_op jit(solution)/shard_map/all_to_all | solution.py:73
Sparse Core Ops, SparseCore 0:
  20.2 54.4 all-gather.3
  102.2 19.2 all-gather.5
where the time goes:
time: 156 us; the launch traced here: 155 us
  waiting for transfers between devices  58.8 us (38%)
  starting transfers between devices  35 us (22%)
  local copies, waits for them, and re-layouts  15.4 us (10%)
  matrix products  13.8 us (9%)
  between operations  13.5 us (9%)
  blocking collectives  12.8 us (8%)
  other arithmetic  2.86 us (2%)
  loops' own time  2.77 us (2%)
    all_to_all x1, starting transfers between devices, shards(): lax.all_to_all(queries[0], 'sp', split_axis=1, concat_axis=0, tiled=True)  18.9 us
    all_to_all x1, waiting for transfers between devices, shards(): lax.all_to_all(values[0], 'sp', split_axis=1, concat_axis=0, tiled=True)  16.6 us
    all_to_all x1, waiting for transfers between devices, shards(): lax.all_to_all(keys[0], 'sp', split_axis=1, concat_axis=0, tiled=True)  14.6 us
    all_to_all x1, waiting for transfers between devices, shards(): lax.all_to_all(queries[0], 'sp', split_axis=1, concat_axis=0, tiled=True)  14.5 us
    all_to_all x1, waiting for transfers between devices, shards(): lax.all_to_all(head_out, 'sp', split_axis=0, concat_axis=1, tiled=True)  13 us
    all_gather x1, blocking collectives, gather_in_order(): blocks = lax.all_gather(blocks, axes[k], axis=0, tiled=True)  12.8 us
    unnamed x8, local copies, waits for them, and re-layouts  6.23 us
    all_to_all x1, starting transfers between devices, shards(): lax.all_to_all(values[0], 'sp', split_axis=1, concat_axis=0, tiled=True)  5.56 us
  transfers between devices with their start and end apart: 6, of which 4 were waited for; matrix products, arithmetic and copies ran while one was open for 17% of the time, Pallas kernels for 0%

commit v1 on v0

v1 whole, which is shorter than its diff:
```python
import jax
import jax.numpy as jnp
from jax import lax
from jax.experimental import pallas as pl
from jax.experimental.pallas import tpu as pltpu
from jax.sharding import Mesh
from jax.sharding import PartitionSpec as P


DP = ("dp_0", "dp_1", "dp_2")
VMEM = pl.BlockSpec(memory_space=pltpu.VMEM)
SMEM = pl.BlockSpec(memory_space=pltpu.SMEM)


def pack_kernel(q_hbm, k_hbm, v_hbm, out_ref, q_ref, k_ref, v_ref, sems):
    rows, width = q_ref.shape
    half = 64
    copies = [
        pltpu.make_async_copy(src.at[0], dst, sems.at[n])
        for n, (src, dst) in enumerate(((k_hbm, k_ref), (v_hbm, v_ref), (q_hbm, q_ref)))
    ]
    for copy in copies:
        copy.start()
    copies[0].wait()
    for j in range(width // 128):
        turned = k_ref[:, j * 128 : (j + 1) * 128].T
        out_ref[2 * j, rows:, :] = turned[:half]
        out_ref[2 * j + 1, rows:, :] = turned[half:]
    copies[1].wait()
    copies[2].wait()
    for j in range(width // 128):
        cols = slice(j * 128, (j + 1) * 128)
        q, v = q_ref[:, cols] * jnp.bfloat16(0.125), v_ref[:, cols]
        out_ref[2 * j, 0:rows, :] = jnp.concatenate([v[:, :half], q[:, :half]], axis=1)
        out_ref[2 * j + 1, 0:rows, :] = jnp.concatenate([v[:, half:], q[:, half:]], axis=1)


def pack(queries, keys, values):
    return pl.pallas_call(
        pack_kernel,
        out_shape=pltpu.VMEM((16, 192, 128), jnp.bfloat16),
        in_specs=[pl.BlockSpec(memory_space=pltpu.HBM)] * 3,
        out_specs=VMEM,
        scratch_shapes=[pltpu.VMEM((128, 1024), jnp.bfloat16)] * 3 + [pltpu.SemaphoreType.DMA((3,))],
    )(queries, keys, values)


def attend_kernel(x_ref, cum_ref, out_ref, keys_ref, vals_ref):
    blocks = x_ref.shape[0]
    length = blocks * 128
    keys_ref[0:64, :] = jnp.zeros((64, length), jnp.bfloat16)
    vals_ref[:, 128:] = jnp.ones((length, 128), jnp.bfloat16)
    for p in range(blocks):
        keys_ref[64:128, p * 128 : (p + 1) * 128] = x_ref[p, 128:192, :]
        vals_ref[p * 128 : (p + 1) * 128, 0:128] = x_ref[p, 0:128, :]
    step = 256
    row = lax.broadcasted_iota(jnp.int32, (step, step), 0)
    col = lax.broadcasted_iota(jnp.int32, (step, step), 1)
    for i in range(length // step):
        here, upto = slice(i * step, (i + 1) * step), (i + 1) * step
        scores = jnp.dot(
            vals_ref[here, 0:128], keys_ref[:, :upto], preferred_element_type=jnp.float32
        )
        scores = scores - cum_ref[:, :upto]
        last = jnp.where(col <= row, scores[:, upto - step :], -jnp.inf)
        scores = jnp.concatenate([scores[:, : upto - step], last], axis=1) if i else last
        top = jnp.max(scores, axis=1, keepdims=True)
        expon = jnp.exp(scores - top).astype(jnp.bfloat16)
        both = jnp.dot(expon, vals_ref[:upto, :], preferred_element_type=jnp.float32)
        head = (both[:, :128] / both[:, 128:]).astype(jnp.bfloat16).T
        out_ref[2 * i] = head[0:64, 0:128]
        out_ref[2 * i + 1] = head[0:64, 128:256]


def attend(packed, cum):
    length = cum.shape[1]
    return pl.pallas_call(
        attend_kernel,
        out_shape=pltpu.VMEM((16, 64, 128), jnp.bfloat16),
        in_specs=[VMEM] * 2,
        out_specs=VMEM,
        scratch_shapes=[
            pltpu.VMEM((128, length), jnp.bfloat16),
            pltpu.VMEM((length, 256), jnp.bfloat16),
        ],
        compiler_params=pltpu.CompilerParams(vmem_limit_bytes=28 << 20),
    )(packed, cum)


def project_kernel(base_ref, head_ref, *refs):
    *parts, out_ref, turned_ref = refs
    heads = head_ref[...]
    for n, part in enumerate(parts):
        rows = jnp.dot(part[...], heads, preferred_element_type=jnp.float32)
        for y in range(8):
            place = pl.multiple_of(base_ref[n] + base_ref[len(parts) + y], 32)
            turned_ref[pl.ds(place, 32), :] = rows[y * 32 : (y + 1) * 32]
    for n in range(out_ref.shape[1] // 128):
        cols = slice(n * 128, (n + 1) * 128)
        out_ref[:, cols] = turned_ref[cols, :].astype(jnp.bfloat16).T


def project(heads, parts, bases):
    return pl.pallas_call(
        project_kernel,
        out_shape=jax.ShapeDtypeStruct((128, 2048), jnp.bfloat16),
        in_specs=[SMEM] + [VMEM] * (1 + len(parts)),
        out_specs=VMEM,
        scratch_shapes=[pltpu.VMEM((2048, 128), jnp.float32)],
        compiler_params=pltpu.CompilerParams(vmem_limit_bytes=12 << 20),
    )(bases, heads, *parts)


def shift(value, axis, by):
    n = lax.axis_size(axis)
    return lax.ppermute(value, axis, [(s, (s + by) % n) for s in range(n)])


def gather_weight(out_weight):
    y, x, core = (lax.axis_index(axis) for axis in DP)
    rows = out_weight.T
    for by in (4, 2, 1):
        rows = jnp.concatenate([rows, shift(rows, "dp_0", by)])
    there = [(i * 2 + c, (i + 1 - 2 * c) % 4 * 2 + c) for i in range(4) for c in range(2)]
    back = [(target, source) for source, target in there]
    near = [lax.ppermute(rows, DP[1:], way) for way in (there, back)]
    far = lax.ppermute(near[0], DP[1:], there)
    pieces = [rows, *near, far]
    others = [shift(rows, "dp_2", 1)]
    others += [shift(piece, "dp_2", 1) for piece in pieces[1:]]
    cores = core ^ jnp.array([0, 0, 0, 0, 1, 1, 1, 1], jnp.int32)
    owners = (x + jnp.array([0, -1, 1, 2] * 2, jnp.int32) * (1 - 2 * cores)) & 3
    places = (y - jnp.array([0, 4, 2, 6, 1, 5, 3, 7], jnp.int32)) & 7
    return pieces + others, jnp.concatenate([(owners * 2 + cores) * 32, places * 256])


def shards(queries, keys, values, cum_gates, out_weight):
    packed = pack(queries, keys, values)
    packed = lax.all_to_all(packed, "sp", split_axis=0, concat_axis=0, tiled=True)
    parts, bases = gather_weight(out_weight)
    heads = attend(packed, cum_gates[0])
    heads = lax.all_to_all(heads, "sp", split_axis=0, concat_axis=0, tiled=True)
    return project(heads.reshape(1024, 128), parts, bases)[None]


def solution(mesh):
    split = Mesh(mesh.devices.reshape(mesh.shape["sp"], 8, 4, 2), ("sp", "dp_0", "dp_1", "dp_2"))
    placed = (
        P(DP, "sp", None),
        P(DP, "sp", None),
        P(DP, "sp", None),
        P(DP, "sp", None),
        P(None, DP),
    )
    return jax.shard_map(
        shards, mesh=split, in_specs=placed, out_specs=P(DP, "sp", None), check_vma=False
    )
```

time: 156 us -> 110 us (0.71)
  the two profiles are of different devices: /device:TPU:56 before, /device:TPU:32 now
where the time goes in v1:
time: 110 us; the launch traced here: 109 us
  starting transfers between devices  58.9 us (54%)
  waiting for transfers between devices  38.4 us (35%)
  Pallas kernels  11 us (10%)
    ppermute x7, waiting for transfers between devices, shift(): return lax.ppermute(value, axis, [(s, (s + by) % n) for s in range(n)])  22.4 us
    all_to_all x1, starting transfers between devices, shards(): lax.all_to_all(packed, 'sp', split_axis=0, concat_axis=0, tiled=True)  19 us
    ppermute x7, starting transfers between devices, shift(): return lax.ppermute(value, axis, [(s, (s + by) % n) for s in range(n)])  17 us
    all_to_all x1, starting transfers between devices, shards(): heads = lax.all_to_all(heads, 'sp', split_axis=0, concat_axis=0, tiled=True)  13.1 us
    ppermute x2, waiting for transfers between devices, gather_weight(): near = [lax.ppermute(rows, DP[1:], way) for way in (there, back)]  9.93 us
    ppermute x2, starting transfers between devices, gather_weight(): near = [lax.ppermute(rows, DP[1:], way) for way in (there, back)]  7.05 us
    all_to_all x1, waiting for transfers between devices, shards(): heads = lax.all_to_all(heads, 'sp', split_axis=0, concat_axis=0, tiled=True)  6.1 us
    pallas_call x1, Pallas kernels, attend(): pl.pallas_call(attend_kernel, out_shape=pltpu.VMEM((16, 64, 128), jnp.bfl...  5.36 us
  transfers between devices with their start and end apart: 12, of which 6 were waited for; matrix products, arithmetic and copies ran while one was open for 0% of the time, Pallas kernels for 5%

profile of v1, /device:TPU:32, one launch (start us, length us, event | category | flops | bytes accessed | tf_op | source)
XLA Modules:
  0.0 109.3 jit_solution(13353384832782047623)
XLA Ops:
  0.0 2.2 %shard_map.82 = bf16[16,192,128]{2,1,0:T(8,128)(2,1)} custom-call(bf16[1,128,1024]{2,1,0:T(8,128)(2,1)} %q_hbm.1, bf16[1,128,1024]{2,1,0:T(8,128)(2,1)} %k_hbm.1, bf16[1,128,1024]{2,1,0:T(8,128)(2,1)} %v_hbm.1), custom_call_target="tpu_custom_call" | custom-call | tf_op jit(solution)/shard_map/pallas_call | solution.py:39
  2.2 19.0 %all-to-all-start = ((bf16[16,192,128]{2,1,0:T(8,128)(2,1)}), bf16[16,192,128]{2,1,0:T(8,128)(2,1)S(1)}, u32[]{:S(2)}, u32[]{:S(2)}) async-start(bf16[16,192,128]{2,1,0:T(8,128)(2,1)} %shard_map.82), calls=%async_computation | async-start | bytes 1572864 | tf_op jit(solution)/shard_map/all_to_all | solution.py:139
  21.3 2.0 %collective-permute-start = (bf16[32,1024]{1,0:T(8,128)(2,1)S(1)}, bf16[32,1024]{1,0:T(8,128)(2,1)S(1)}, u32[]{:S(2)}, u32[]{:S(2)}) collective-permute-start(bf16[32,1024]{1,0:T(8,128)(2,1)S(1)} %bitcast.6), channel_id=1, source_target_pairs={{0,32},{8,40},{16,48},{24,56},{32,0},{40,8},{48,16},{56,24},{1,33}... | collective-permute-start | bytes 196616 | tf_op jit(solution)/shard_map/ppermute | solution.py:116
  23.3 8.8 %collective-permute-done = bf16[32,1024]{1,0:T(8,128)(2,1)S(1)} collective-permute-done((bf16[32,1024]{1,0:T(8,128)(2,1)S(1)}, bf16[32,1024]{1,0:T(8,128)(2,1)S(1)}, u32[]{:S(2)}, u32[]{:S(2)}) %collective-permute-start) | collective-permute-done | bytes 65568 | tf_op jit(solution)/shard_map/ppermute | solution.py:116
  32.1 2.5 %collective-permute-start.1 = (bf16[64,1024]{1,0:T(8,128)(2,1)S(1)}, bf16[64,1024]{1,0:T(8,128)(2,1)S(1)}, u32[]{:S(2)}, u32[]{:S(2)}) collective-permute-start(bf16[64,1024]{1,0:T(8,128)(2,1)S(1)} %pad_maximum_fusion.2), channel_id=1, source_target_pairs={{0,16},{8,24},{16,32},{24,40},{32,48},{40,56},{48,0},{56,8},{1,17}... | collective-permute-start | bytes 393224 | tf_op jit(solution)/shard_map/ppermute | solution.py:116
  34.6 6.9 %collective-permute-done.1 = bf16[64,1024]{1,0:T(8,128)(2,1)S(1)} collective-permute-done((bf16[64,1024]{1,0:T(8,128)(2,1)S(1)}, bf16[64,1024]{1,0:T(8,128)(2,1)S(1)}, u32[]{:S(2)}, u32[]{:S(2)}) %collective-permute-start.1) | collective-permute-done | bytes 131104 | tf_op jit(solution)/shard_map/ppermute | solution.py:116
  41.5 3.8 %collective-permute-start.2 = (bf16[128,1024]{1,0:T(8,128)(2,1)S(1)}, bf16[128,1024]{1,0:T(8,128)(2,1)S(1)}, u32[]{:S(2)}, u32[]{:S(2)}) collective-permute-start(bf16[128,1024]{1,0:T(8,128)(2,1)S(1)} %pad_maximum_fusion.1), channel_id=1, source_target_pairs={{0,8},{8,16},{16,24},{24,32},{32,40},{40,48},{48,56},{56,0},{1,9},... | collective-permute-start | bytes 786440 | tf_op jit(solution)/shard_map/ppermute | solution.py:116
  45.3 5.8 %collective-permute-done.2 = bf16[128,1024]{1,0:T(8,128)(2,1)S(1)} collective-permute-done((bf16[128,1024]{1,0:T(8,128)(2,1)S(1)}, bf16[128,1024]{1,0:T(8,128)(2,1)S(1)}, u32[]{:S(2)}, u32[]{:S(2)}) %collective-permute-start.2) | collective-permute-done | bytes 262176 | tf_op jit(solution)/shard_map/ppermute | solution.py:116
  51.2 3.4 %collective-permute-start.3 = (bf16[256,1024]{1,0:T(8,128)(2,1)S(1)}, bf16[256,1024]{1,0:T(8,128)(2,1)S(1)}, u32[]{:S(2)}, u32[]{:S(2)}) collective-permute-start(bf16[256,1024]{1,0:T(8,128)(2,1)S(1)} %pad_maximum_fusion.refs_0_), channel_id=1, source_target_pairs={{0,2},{1,7},{2,4},{3,1},{4,6},{5,3},{6,0},{7,5},{8,10},{9,15},{10,... | collective-permute-start | bytes 1572872 | tf_op jit(solution)/shard_map/ppermute | solution.py:126
  54.6 3.7 %collective-permute-start.4 = (bf16[256,1024]{1,0:T(8,128)(2,1)S(1)}, bf16[256,1024]{1,0:T(8,128)(2,1)S(1)}, u32[]{:S(2)}, u32[]{:S(2)}) collective-permute-start(bf16[256,1024]{1,0:T(8,128)(2,1)S(1)} %pad_maximum_fusion.refs_0_), channel_id=1, source_target_pairs={{2,0},{7,1},{4,2},{1,3},{6,4},{3,5},{0,6},{5,7},{10,8},{15,9},{12,... | collective-permute-start | bytes 1572872 | tf_op jit(solution)/shard_map/ppermute | solution.py:126
  58.3 9.9 %collective-permute-done.3.refs_1_ = bf16[256,1024]{1,0:T(8,128)(2,1)S(1)} collective-permute-done((bf16[256,1024]{1,0:T(8,128)(2,1)S(1)}, bf16[256,1024]{1,0:T(8,128)(2,1)S(1)}, u32[]{:S(2)}, u32[]{:S(2)}) %collective-permute-start.3) | collective-permute-done | bytes 524320 | tf_op jit(solution)/shard_map/ppermute | solution.py:126
  68.2 2.8 %collective-permute-start.5 = (bf16[256,1024]{1,0:T(8,128)(2,1)S(1)}, bf16[256,1024]{1,0:T(8,128)(2,1)S(1)}, u32[]{:S(2)}, u32[]{:S(2)}) collective-permute-start(bf16[256,1024]{1,0:T(8,128)(2,1)S(1)} %collective-permute-done.3.refs_1_), channel_id=1, source_target_pairs={{0,2},{1,7},{2,4},{3,1},{4,6},{5,3},{6,0},{7,5},{8,10},{9,15},{10,... | collective-permute-start | bytes 1572872 | tf_op jit(solution)/shard_map/ppermute | solution.py:127
  71.0 5.4 %shard_map.83 = bf16[16,64,128]{2,1,0:T(8,128)(2,1)} custom-call(bf16[16,192,128]{2,1,0:T(8,128)(2,1)S(1)} %all-to-all-done.x_ref, f32[1,2048]{1,0:T(1,128)S(1)} %bitcast.5), custom_call_target="tpu_custom_call" | custom-call | tf_op jit(solution)/shard_map/pallas_call | solution.py:77
  76.4 13.1 %all-to-all-start.1 = ((bf16[16,64,128]{2,1,0:T(8,128)(2,1)}), bf16[16,64,128]{2,1,0:T(8,128)(2,1)S(1)}, u32[]{:S(2)}, u32[]{:S(2)}) async-start(bf16[16,64,128]{2,1,0:T(8,128)(2,1)} %shard_map.83), calls=%async_computation.1 | async-start | bytes 524288 | tf_op jit(solution)/shard_map/all_to_all | solution.py:142
  89.5 1.9 %collective-permute-start.6 = (bf16[256,1024]{1,0:T(8,128)(2,1)S(1)}, bf16[256,1024]{1,0:T(8,128)(2,1)S(1)}, u32[]{:S(2)}, u32[]{:S(2)}) collective-permute-start(bf16[256,1024]{1,0:T(8,128)(2,1)S(1)} %pad_maximum_fusion.refs_0_), channel_id=1, source_target_pairs={{0,1},{1,0},{2,3},{3,2},{4,5},{5,4},{6,7},{7,6},{8,9},{9,8},{10,11... | collective-permute-start | bytes 1572872 | tf_op jit(solution)/shard_map/ppermute | solution.py:116
  91.4 2.4 %collective-permute-start.7 = (bf16[256,1024]{1,0:T(8,128)(2,1)S(1)}, bf16[256,1024]{1,0:T(8,128)(2,1)S(1)}, u32[]{:S(2)}, u32[]{:S(2)}) collective-permute-start(bf16[256,1024]{1,0:T(8,128)(2,1)S(1)} %collective-permute-done.3.refs_1_), channel_id=1, source_target_pairs={{0,1},{1,0},{2,3},{3,2},{4,5},{5,4},{6,7},{7,6},{8,9},{9,8},{10,11... | collective-permute-start | bytes 1572872 | tf_op jit(solution)/shard_map/ppermute | solution.py:116
  93.8 1.9 %collective-permute-start.8 = (bf16[256,1024]{1,0:T(8,128)(2,1)S(1)}, bf16[256,1024]{1,0:T(8,128)(2,1)}, u32[]{:S(2)}, u32[]{:S(2)}) collective-permute-start(bf16[256,1024]{1,0:T(8,128)(2,1)S(1)} %collective-permute-done.4.refs_2_), channel_id=1, source_target_pairs={{0,1},{1,0},{2,3},{3,2},{4,5},{5,4},{6,7},{7,6},{8,9},{9,8},{10,11... | collective-permute-start | bytes 1572872 | tf_op jit(solution)/shard_map/ppermute | solution.py:116
  95.8 2.4 %collective-permute-start.9 = (bf16[256,1024]{1,0:T(8,128)(2,1)S(1)}, bf16[256,1024]{1,0:T(8,128)(2,1)}, u32[]{:S(2)}, u32[]{:S(2)}) collective-permute-start(bf16[256,1024]{1,0:T(8,128)(2,1)S(1)} %collective-permute-done.5.refs_3_), channel_id=1, source_target_pairs={{0,1},{1,0},{2,3},{3,2},{4,5},{5,4},{6,7},{7,6},{8,9},{9,8},{10,11... | collective-permute-start | bytes 1572872 | tf_op jit(solution)/shard_map/ppermute | solution.py:116
  98.2 0.6 copy-done.2
  98.8 0.0 copy-done.3
  98.9 0.1 pad_add_fusion.base_ref
  99.0 0.8 collective-permute-done.9.refs_7_
  99.8 6.1 %all-to-all-done.1 = bf16[16,64,128]{2,1,0:T(8,128)(2,1)S(1)} async-done(((bf16[16,64,128]{2,1,0:T(8,128)(2,1)}), bf16[16,64,128]{2,1,0:T(8,128)(2,1)S(1)}, u32[]{:S(2)}, u32[]{:S(2)}) %all-to-all-start.1) | async-done | bytes 262176 | tf_op jit(solution)/shard_map/all_to_all | solution.py:142
  105.9 3.4 %shard_map.84 = bf16[128,2048]{1,0:T(8,128)(2,1)} custom-call(s32[16]{0:T(128)S(1)} %pad_add_fusion.base_ref, bf16[1024,128]{1,0:T(8,128)(2,1)S(1)} %bitcast.4, bf16[256,1024]{1,0:T(8,128)(2,1)S(1)} %pad_maximum_fusion.refs_0_, bf16[256,1024]{1,0:T(8,128)(2,1)S(1)} %collective-permute-done.3.refs_1_, bf16[256,1024]{1,0:T(8,128)(2,1)S(1)} %collective-permute-done.4.refs_2_, ...), custom_call_target="tpu_custom_call" | custom-call | tf_op jit(solution)/shard_map/pallas_call | solution.py:104
  (18 shorter events, 0.1 us)
Async XLA Ops:
  2.2 19.0 %copy-start.1 = (bf16[1024,32]{0,1:T(8,128)(2,1)S(1)}, bf16[1024,32]{0,1:T(8,128)(2,1)}, u32[]{:S(2)}) copy-start(bf16[1024,32]{0,1:T(8,128)(2,1)} %param.12) | copy-start | bytes 196612
  2.2 68.8 %all-to-all-start = ((bf16[16,192,128]{2,1,0:T(8,128)(2,1)}), bf16[16,192,128]{2,1,0:T(8,128)(2,1)S(1)}, u32[]{:S(2)}, u32[]{:S(2)}) async-start(bf16[16,192,128]{2,1,0:T(8,128)(2,1)} %shard_map.82), calls=%async_computation | async-start | bytes 1572864 | tf_op jit(solution)/shard_map/all_to_all | solution.py:139
  21.3 10.8 %collective-permute-start = (bf16[32,1024]{1,0:T(8,128)(2,1)S(1)}, bf16[32,1024]{1,0:T(8,128)(2,1)S(1)}, u32[]{:S(2)}, u32[]{:S(2)}) collective-permute-start(bf16[32,1024]{1,0:T(8,128)(2,1)S(1)} %bitcast.6), channel_id=1, source_target_pairs={{0,32},{8,40},{16,48},{24,56},{32,0},{40,8},{48,16},{56,24},{1,33}... | collective-permute-start | bytes 196616 | tf_op jit(solution)/shard_map/ppermute | solution.py:116
  32.1 9.3 %collective-permute-start.1 = (bf16[64,1024]{1,0:T(8,128)(2,1)S(1)}, bf16[64,1024]{1,0:T(8,128)(2,1)S(1)}, u32[]{:S(2)}, u32[]{:S(2)}) collective-permute-start(bf16[64,1024]{1,0:T(8,128)(2,1)S(1)} %pad_maximum_fusion.2), channel_id=1, source_target_pairs={{0,16},{8,24},{16,32},{24,40},{32,48},{40,56},{48,0},{56,8},{1,17}... | collective-permute-start | bytes 393224 | tf_op jit(solution)/shard_map/ppermute | solution.py:116
  41.5 29.5 %copy-start = (f32[1,1,2048]{2,1,0:T(1,128)S(1)}, f32[1,1,2048]{2,1,0:T(1,128)}, u32[]{:S(2)}) copy-start(f32[1,1,2048]{2,1,0:T(1,128)} %param.11) | copy-start | bytes 24580
  41.5 9.7 %collective-permute-start.2 = (bf16[128,1024]{1,0:T(8,128)(2,1)S(1)}, bf16[128,1024]{1,0:T(8,128)(2,1)S(1)}, u32[]{:S(2)}, u32[]{:S(2)}) collective-permute-start(bf16[128,1024]{1,0:T(8,128)(2,1)S(1)} %pad_maximum_fusion.1), channel_id=1, source_target_pairs={{0,8},{8,16},{16,24},{24,32},{32,40},{40,48},{48,56},{56,0},{1,9},... | collective-permute-start | bytes 786440 | tf_op jit(solution)/shard_map/ppermute | solution.py:116
  51.2 17.0 %collective-permute-start.3 = (bf16[256,1024]{1,0:T(8,128)(2,1)S(1)}, bf16[256,1024]{1,0:T(8,128)(2,1)S(1)}, u32[]{:S(2)}, u32[]{:S(2)}) collective-permute-start(bf16[256,1024]{1,0:T(8,128)(2,1)S(1)} %pad_maximum_fusion.refs_0_), channel_id=1, source_target_pairs={{0,2},{1,7},{2,4},{3,1},{4,6},{5,3},{6,0},{7,5},{8,10},{9,15},{10,... | collective-permute-start | bytes 1572872 | tf_op jit(solution)/shard_map/ppermute | solution.py:126
  54.6 39.2 %collective-permute-start.4 = (bf16[256,1024]{1,0:T(8,128)(2,1)S(1)}, bf16[256,1024]{1,0:T(8,128)(2,1)S(1)}, u32[]{:S(2)}, u32[]{:S(2)}) collective-permute-start(bf16[256,1024]{1,0:T(8,128)(2,1)S(1)} %pad_maximum_fusion.refs_0_), channel_id=1, source_target_pairs={{2,0},{7,1},{4,2},{1,3},{6,4},{3,5},{0,6},{5,7},{10,8},{15,9},{12,... | collective-permute-start | bytes 1572872 | tf_op jit(solution)/shard_map/ppermute | solution.py:126
  68.2 27.6 %collective-permute-start.5 = (bf16[256,1024]{1,0:T(8,128)(2,1)S(1)}, bf16[256,1024]{1,0:T(8,128)(2,1)S(1)}, u32[]{:S(2)}, u32[]{:S(2)}) collective-permute-start(bf16[256,1024]{1,0:T(8,128)(2,1)S(1)} %collective-permute-done.3.refs_1_), channel_id=1, source_target_pairs={{0,2},{1,7},{2,4},{3,1},{4,6},{5,3},{6,0},{7,5},{8,10},{9,15},{10,... | collective-permute-start | bytes 1572872 | tf_op jit(solution)/shard_map/ppermute | solution.py:127
  76.4 29.5 %all-to-all-start.1 = ((bf16[16,64,128]{2,1,0:T(8,128)(2,1)}), bf16[16,64,128]{2,1,0:T(8,128)(2,1)S(1)}, u32[]{:S(2)}, u32[]{:S(2)}) async-start(bf16[16,64,128]{2,1,0:T(8,128)(2,1)} %shard_map.83), calls=%async_computation.1 | async-start | bytes 524288 | tf_op jit(solution)/shard_map/all_to_all | solution.py:142
  89.5 9.5 %collective-permute-start.6 = (bf16[256,1024]{1,0:T(8,128)(2,1)S(1)}, bf16[256,1024]{1,0:T(8,128)(2,1)S(1)}, u32[]{:S(2)}, u32[]{:S(2)}) collective-permute-start(bf16[256,1024]{1,0:T(8,128)(2,1)S(1)} %pad_maximum_fusion.refs_0_), channel_id=1, source_target_pairs={{0,1},{1,0},{2,3},{3,2},{4,5},{5,4},{6,7},{7,6},{8,9},{9,8},{10,11... | collective-permute-start | bytes 1572872 | tf_op jit(solution)/shard_map/ppermute | solution.py:116
  91.4 7.6 %collective-permute-start.7 = (bf16[256,1024]{1,0:T(8,128)(2,1)S(1)}, bf16[256,1024]{1,0:T(8,128)(2,1)S(1)}, u32[]{:S(2)}, u32[]{:S(2)}) collective-permute-start(bf16[256,1024]{1,0:T(8,128)(2,1)S(1)} %collective-permute-done.3.refs_1_), channel_id=1, source_target_pairs={{0,1},{1,0},{2,3},{3,2},{4,5},{5,4},{6,7},{7,6},{8,9},{9,8},{10,11... | collective-permute-start | bytes 1572872 | tf_op jit(solution)/shard_map/ppermute | solution.py:116
  93.8 5.2 %collective-permute-start.8 = (bf16[256,1024]{1,0:T(8,128)(2,1)S(1)}, bf16[256,1024]{1,0:T(8,128)(2,1)}, u32[]{:S(2)}, u32[]{:S(2)}) collective-permute-start(bf16[256,1024]{1,0:T(8,128)(2,1)S(1)} %collective-permute-done.4.refs_2_), channel_id=1, source_target_pairs={{0,1},{1,0},{2,3},{3,2},{4,5},{5,4},{6,7},{7,6},{8,9},{9,8},{10,11... | collective-permute-start | bytes 1572872 | tf_op jit(solution)/shard_map/ppermute | solution.py:116
  95.8 4.1 %collective-permute-start.9 = (bf16[256,1024]{1,0:T(8,128)(2,1)S(1)}, bf16[256,1024]{1,0:T(8,128)(2,1)}, u32[]{:S(2)}, u32[]{:S(2)}) collective-permute-start(bf16[256,1024]{1,0:T(8,128)(2,1)S(1)} %collective-permute-done.5.refs_3_), channel_id=1, source_target_pairs={{0,1},{1,0},{2,3},{3,2},{4,5},{5,4},{6,7},{7,6},{8,9},{9,8},{10,11... | collective-permute-start | bytes 1572872 | tf_op jit(solution)/shard_map/ppermute | solution.py:116
  98.2 0.7 copy-start.2
  98.2 0.7 copy-start.3
  98.2 0.7 copy-start.4

commit v2 on v1

v2 whole, which is shorter than its diff:
```python
import jax
import jax.numpy as jnp
from jax import lax
from jax.experimental import pallas as pl
from jax.experimental.pallas import tpu as pltpu
from jax.sharding import Mesh
from jax.sharding import PartitionSpec as P


DP = ("dp_0", "dp_1", "dp_2")
VMEM = pl.BlockSpec(memory_space=pltpu.VMEM)
SMEM = pl.BlockSpec(memory_space=pltpu.SMEM)
HBM = pl.BlockSpec(memory_space=pltpu.HBM)
STEP, PART = 256, 128


def pack_kernel(q_hbm, k_hbm, v_hbm, out_hbm, q_ref, k_ref, v_ref, out_ref, sems):
    _, width = q_ref.shape
    half = 64
    copies = [
        pltpu.make_async_copy(src.at[0], dst, sems.at[n])
        for n, (src, dst) in enumerate(((q_hbm, q_ref), (v_hbm, v_ref), (k_hbm, k_ref)))
    ]
    for copy in copies:
        copy.start()

    def send(n):
        third = pl.ds(n * half, half)
        copies.append(
            pltpu.make_async_copy(out_ref.at[:, third], out_hbm.at[:, third], sems.at[3 + n])
        )
        copies[-1].start()

    copies[0].wait()
    for j in range(width // 128):
        turned = (q_ref[:, j * 128 : (j + 1) * 128] * jnp.bfloat16(0.125)).T
        out_ref[2 * j, 0:half, :] = turned[:half]
        out_ref[2 * j + 1, 0:half, :] = turned[half:]
    send(0)
    copies[1].wait()
    for j in range(width // 128):
        turned = v_ref[:, j * 128 : (j + 1) * 128].T
        out_ref[2 * j, half : 2 * half, :] = turned[:half]
        out_ref[2 * j + 1, half : 2 * half, :] = turned[half:]
    send(1)
    copies[2].wait()
    for j in range(width // 128):
        k = k_ref[:, j * 128 : (j + 1) * 128]
        out_ref[2 * j, 2 * half :, :] = jnp.concatenate([k[:half, :half], k[half:, :half]], axis=1)
        out_ref[2 * j + 1, 2 * half :, :] = jnp.concatenate([k[:half, half:], k[half:, half:]], axis=1)
    send(2)
    for copy in copies[3:]:
        copy.wait()


def pack(queries, keys, values):
    return pl.pallas_call(
        pack_kernel,
        out_shape=jax.ShapeDtypeStruct((16, 192, 128), jnp.bfloat16),
        in_specs=[HBM] * 3,
        out_specs=HBM,
        scratch_shapes=[pltpu.VMEM((128, 1024), jnp.bfloat16)] * 3
        + [pltpu.VMEM((16, 192, 128), jnp.bfloat16), pltpu.SemaphoreType.DMA((6,))],
    )(queries, keys, values)


def attend_kernel(x_ref, cum_ref, out_hbm, out_ref, sems, keys_ref, queries_ref, values_ref, score_ref, expon_ref):
    blocks = x_ref.shape[0]
    length = blocks * 128
    tiles = length // STEP
    lane = lax.broadcasted_iota(jnp.int32, (64, 128), 1)
    row = lax.broadcasted_iota(jnp.int32, (PART, STEP), 0)
    col = lax.broadcasted_iota(jnp.int32, (PART, STEP), 1)

    gates = -cum_ref[...]
    high = gates.astype(jnp.bfloat16).astype(jnp.float32)
    mid = (gates - high).astype(jnp.bfloat16).astype(jnp.float32)
    low = gates - high - mid
    blank = jnp.zeros((64, 128), jnp.float32)
    turned = jnp.concatenate([blank, high, mid, low, blank[:16]], axis=0).T.astype(jnp.bfloat16)
    queries_ref[64:112, :] = jnp.ones((48, length), jnp.bfloat16)
    queries_ref[112:, :] = jnp.zeros((16, length), jnp.bfloat16)
    values_ref[64:, :] = jnp.ones((16, length), jnp.bfloat16)
    nothing = jnp.zeros((64, 128), jnp.bfloat16)
    for p in range(blocks):
        spot = slice(p * 128, (p + 1) * 128)
        queries_ref[0:64, spot] = x_ref[p, 0:64, :]
        values_ref[0:64, spot] = x_ref[p, 64:128, :]
        both = x_ref[p, 128:192, :]
        other = jnp.concatenate([both[:, 64:], both[:, :64]], axis=1)
        for keys, part in ((both, 0), (other, 64)):
            gate = jnp.where((lane & 15) == p, turned[part : part + 64], nothing)
            keys_ref[p * 128 + part : p * 128 + part + 64, :] = jnp.where(lane < 64, keys, gate)

    def score(i, s, top):
        scores = jnp.dot(keys_ref[s : s + PART, :], queries_ref[:, i * STEP : (i + 1) * STEP], preferred_element_type=jnp.float32)
        if s >= i * STEP:
            scores = jnp.where(row + (s - i * STEP) <= col, scores, -jnp.inf)
        score_ref[i % 2, s : s + PART, :] = scores
        most = jnp.max(scores.reshape(PART // 8, 8, STEP), axis=0)
        return most if top is None else jnp.maximum(top, most)

    def weigh(i, s, top):
        expon_ref[i % 2, s : s + PART, :] = jnp.exp(score_ref[i % 2, s : s + PART, :] - top).astype(jnp.bfloat16)

    def finish(i):
        upto = (i + 1) * STEP
        both = jnp.dot(values_ref[:, :upto], expon_ref[i % 2, :upto, :], preferred_element_type=jnp.float32)
        head = (both[0:64] / both[64:65]).astype(jnp.bfloat16)
        out_ref[2 * i] = head[:, 0:128]
        out_ref[2 * i + 1] = head[:, 128:256]
        pair = pl.ds(2 * i, 2)
        copies.append(pltpu.make_async_copy(out_ref.at[pair], out_hbm.at[pair], sems.at[i]))
        copies[-1].start()

    copies = []
    tops = {}
    order = list(reversed(range(tiles)))
    for n, i in enumerate(order + [None]):
        before = order[n - 1] if n else None
        todo = list(range(0, (i + 1) * STEP, PART)) if i is not None else []
        late = list(range(0, (before + 1) * STEP, PART)) if n else []
        top = None
        for m in range(max(len(todo), len(late))):
            if m < len(late):
                weigh(before, late[m], tops[before])
            if m < len(todo):
                top = score(i, todo[m], top)
        if top is not None:
            tops[i] = jnp.max(top, axis=0, keepdims=True)
        if n:
            finish(before)
    for copy in copies:
        copy.wait()


def attend(packed, cum):
    length = cum.size
    return pl.pallas_call(
        attend_kernel,
        out_shape=jax.ShapeDtypeStruct((16, 64, 128), jnp.bfloat16),
        in_specs=[VMEM] * 2,
        out_specs=HBM,
        scratch_shapes=[
            pltpu.VMEM((16, 64, 128), jnp.bfloat16),
            pltpu.SemaphoreType.DMA((8,)),
            pltpu.VMEM((length, 128), jnp.bfloat16),
            pltpu.VMEM((128, length), jnp.bfloat16),
            pltpu.VMEM((80, length), jnp.bfloat16),
            pltpu.VMEM((2, length, STEP), jnp.float32),
            pltpu.VMEM((2, length, STEP), jnp.bfloat16),
        ],
        compiler_params=pltpu.CompilerParams(vmem_limit_bytes=28 << 20),
    )(packed, cum)


def project_kernel(base_ref, head_ref, *refs):
    *parts, out_ref, turned_ref = refs
    heads = head_ref[...]
    for n, part in enumerate(parts):
        rows = jnp.dot(part[...], heads, preferred_element_type=jnp.float32)
        for y in range(8):
            place = pl.multiple_of(base_ref[n] + base_ref[len(parts) + y], 32)
            turned_ref[pl.ds(place, 32), :] = rows[y * 32 : (y + 1) * 32]
    for n in range(out_ref.shape[2] // 128):
        cols = slice(n * 128, (n + 1) * 128)
        out_ref[0, :, cols] = turned_ref[cols, :].astype(jnp.bfloat16).T


def project(heads, parts, bases):
    return pl.pallas_call(
        project_kernel,
        out_shape=jax.ShapeDtypeStruct((1, 128, 2048), jnp.bfloat16),
        in_specs=[SMEM] + [VMEM] * 9,
        out_specs=VMEM,
        scratch_shapes=[pltpu.VMEM((2048, 128), jnp.float32)],
        compiler_params=pltpu.CompilerParams(vmem_limit_bytes=12 << 20),
    )(bases, heads, *parts)


def shift(value, axis, by):
    n = lax.axis_size(axis)
    return lax.ppermute(value, axis, [(s, (s + by) % n) for s in range(n)])


def gather_weight(out_weight):
    y, x, core = (lax.axis_index(axis) for axis in DP)
    rows = out_weight.T
    for by in (4, 2, 1):
        rows = jnp.concatenate([rows, shift(rows, "dp_0", by)])
    there = [(i * 2 + c, (i + 1 - 2 * c) % 4 * 2 + c) for i in range(4) for c in range(2)]
    back = [(target, source) for source, target in there]
    near = [lax.ppermute(rows, DP[1:], way) for way in (there, back)]
    far = lax.ppermute(near[0], DP[1:], there)
    pieces = [rows, *near, far]
    others = [shift(rows, "dp_2", 1)]
    others += [shift(piece, "dp_2", 1) for piece in pieces[1:]]
    cores = core ^ jnp.array([0, 0, 0, 0, 1, 1, 1, 1], jnp.int32)
    owners = (x + jnp.array([0, -1, 1, 2] * 2, jnp.int32) * (1 - 2 * cores)) & 3
    places = (y - jnp.array([0, 4, 2, 6, 1, 5, 3, 7], jnp.int32)) & 7
    return pieces + others, jnp.concatenate([(owners * 2 + cores) * 32, places * 256])


def shards(queries, keys, values, cum_gates, out_weight):
    packed = pack(queries, keys, values)
    packed = lax.all_to_all(packed, "sp", split_axis=0, concat_axis=0, tiled=True)
    parts, bases = gather_weight(out_weight)
    heads = attend(packed, cum_gates.reshape(16, 128))
    heads = lax.all_to_all(heads, "sp", split_axis=0, concat_axis=0, tiled=True)
    return project(heads.reshape(1024, 128), parts, bases)


def solution(mesh):
    split = Mesh(mesh.devices.reshape(mesh.shape["sp"], 8, 4, 2), ("sp", "dp_0", "dp_1", "dp_2"))
    placed = (
        P(DP, "sp", None),
        P(DP, "sp", None),
        P(DP, "sp", None),
        P(DP, "sp", None),
        P(None, DP),
    )
    return jax.shard_map(
        shards, mesh=split, in_specs=placed, out_specs=P(DP, "sp", None), check_vma=False
    )
```

time: 110 us -> 108 us (0.982)
  Pallas kernels: 11 us -> 9.46 us
    pallas_call x3, Pallas kernels: 11 us -> 9.46 us  [the longest x1 3.91 us: attend(): pl.pallas_call(attend_kernel, out_shape=jax.ShapeDtypeStruct((16, 64, 128...]
  transfers between devices with their start and end apart: 12 -> 12, of which waited for: 6 -> 6; matrix products, arithmetic and copies ran while one was open for 0% -> 0% of each run, Pallas kernels for 5% -> 4%
where the time goes in v2:
time: 108 us
  starting transfers between devices  58.9 us (55%)
  waiting for transfers between devices  38.4 us (36%)
  Pallas kernels  9.46 us (9%)
    ppermute x7, waiting for transfers between devices, shift(): return lax.ppermute(value, axis, [(s, (s + by) % n) for s in range(n)])  22.4 us
    all_to_all x1, starting transfers between devices, shards(): lax.all_to_all(packed, 'sp', split_axis=0, concat_axis=0, tiled=True)  19 us
    ppermute x7, starting transfers between devices, shift(): return lax.ppermute(value, axis, [(s, (s + by) % n) for s in range(n)])  17 us
    all_to_all x1, starting transfers between devices, shards(): heads = lax.all_to_all(heads, 'sp', split_axis=0, concat_axis=0, tiled=True)  13.1 us
    ppermute x2, waiting for transfers between devices, gather_weight(): near = [lax.ppermute(rows, DP[1:], way) for way in (there, back)]  9.93 us
    ppermute x2, starting transfers between devices, gather_weight(): near = [lax.ppermute(rows, DP[1:], way) for way in (there, back)]  7.05 us
    all_to_all x1, waiting for transfers between devices, shards(): heads = lax.all_to_all(heads, 'sp', split_axis=0, concat_axis=0, tiled=True)  6.1 us
    pallas_call x1, Pallas kernels, attend(): pl.pallas_call(attend_kernel, out_shape=jax.ShapeDtypeStruct((16, 64, 128...  3.91 us
  transfers between devices with their start and end apart: 12, of which 6 were waited for; matrix products, arithmetic and copies ran while one was open for 0% of the time, Pallas kernels for 4%

profile of v2, /device:TPU:32, one launch (start us, length us, event | category | flops | bytes accessed | tf_op | source)
XLA Modules:
  0.0 107.8 jit_solution(14424089819070967150)
XLA Ops:
  0.0 2.1 %shard_map.82 = bf16[16,192,128]{2,1,0:T(8,128)(2,1)} custom-call(bf16[1,128,1024]{2,1,0:T(8,128)(2,1)} %q_hbm.1, bf16[1,128,1024]{2,1,0:T(8,128)(2,1)} %k_hbm.1, bf16[1,128,1024]{2,1,0:T(8,128)(2,1)} %v_hbm.1), custom_call_target="tpu_custom_call" | custom-call | tf_op jit(solution)/shard_map/pallas_call | solution.py:57
  2.1 19.0 %all-to-all-start = ((bf16[16,192,128]{2,1,0:T(8,128)(2,1)}), bf16[16,192,128]{2,1,0:T(8,128)(2,1)S(1)}, u32[]{:S(2)}, u32[]{:S(2)}) async-start(bf16[16,192,128]{2,1,0:T(8,128)(2,1)} %shard_map.82), calls=%async_computation | async-start | bytes 1572864 | tf_op jit(solution)/shard_map/all_to_all | solution.py:206
  21.2 2.0 %collective-permute-start = (bf16[32,1024]{1,0:T(8,128)(2,1)S(1)}, bf16[32,1024]{1,0:T(8,128)(2,1)S(1)}, u32[]{:S(2)}, u32[]{:S(2)}) collective-permute-start(bf16[32,1024]{1,0:T(8,128)(2,1)S(1)} %bitcast.5), channel_id=1, source_target_pairs={{0,32},{8,40},{16,48},{24,56},{32,0},{40,8},{48,16},{56,24},{1,33}... | collective-permute-start | bytes 196616 | tf_op jit(solution)/shard_map/ppermute | solution.py:183
  23.2 8.8 %collective-permute-done = bf16[32,1024]{1,0:T(8,128)(2,1)S(1)} collective-permute-done((bf16[32,1024]{1,0:T(8,128)(2,1)S(1)}, bf16[32,1024]{1,0:T(8,128)(2,1)S(1)}, u32[]{:S(2)}, u32[]{:S(2)}) %collective-permute-start) | collective-permute-done | bytes 65568 | tf_op jit(solution)/shard_map/ppermute | solution.py:183
  32.0 2.5 %collective-permute-start.1 = (bf16[64,1024]{1,0:T(8,128)(2,1)S(1)}, bf16[64,1024]{1,0:T(8,128)(2,1)S(1)}, u32[]{:S(2)}, u32[]{:S(2)}) collective-permute-start(bf16[64,1024]{1,0:T(8,128)(2,1)S(1)} %pad_maximum_fusion.2), channel_id=1, source_target_pairs={{0,16},{8,24},{16,32},{24,40},{32,48},{40,56},{48,0},{56,8},{1,17}... | collective-permute-start | bytes 393224 | tf_op jit(solution)/shard_map/ppermute | solution.py:183
  34.5 6.9 %collective-permute-done.1 = bf16[64,1024]{1,0:T(8,128)(2,1)S(1)} collective-permute-done((bf16[64,1024]{1,0:T(8,128)(2,1)S(1)}, bf16[64,1024]{1,0:T(8,128)(2,1)S(1)}, u32[]{:S(2)}, u32[]{:S(2)}) %collective-permute-start.1) | collective-permute-done | bytes 131104 | tf_op jit(solution)/shard_map/ppermute | solution.py:183
  41.4 3.8 %collective-permute-start.2 = (bf16[128,1024]{1,0:T(8,128)(2,1)S(1)}, bf16[128,1024]{1,0:T(8,128)(2,1)S(1)}, u32[]{:S(2)}, u32[]{:S(2)}) collective-permute-start(bf16[128,1024]{1,0:T(8,128)(2,1)S(1)} %pad_maximum_fusion.1), channel_id=1, source_target_pairs={{0,8},{8,16},{16,24},{24,32},{32,40},{40,48},{48,56},{56,0},{1,9},... | collective-permute-start | bytes 786440 | tf_op jit(solution)/shard_map/ppermute | solution.py:183
  45.2 5.8 %collective-permute-done.2 = bf16[128,1024]{1,0:T(8,128)(2,1)S(1)} collective-permute-done((bf16[128,1024]{1,0:T(8,128)(2,1)S(1)}, bf16[128,1024]{1,0:T(8,128)(2,1)S(1)}, u32[]{:S(2)}, u32[]{:S(2)}) %collective-permute-start.2) | collective-permute-done | bytes 262176 | tf_op jit(solution)/shard_map/ppermute | solution.py:183
  51.1 3.4 %collective-permute-start.3 = (bf16[256,1024]{1,0:T(8,128)(2,1)S(1)}, bf16[256,1024]{1,0:T(8,128)(2,1)S(1)}, u32[]{:S(2)}, u32[]{:S(2)}) collective-permute-start(bf16[256,1024]{1,0:T(8,128)(2,1)S(1)} %pad_maximum_fusion.refs_0_), channel_id=1, source_target_pairs={{0,2},{1,7},{2,4},{3,1},{4,6},{5,3},{6,0},{7,5},{8,10},{9,15},{10,... | collective-permute-start | bytes 1572872 | tf_op jit(solution)/shard_map/ppermute | solution.py:193
  54.5 3.7 %collective-permute-start.4 = (bf16[256,1024]{1,0:T(8,128)(2,1)S(1)}, bf16[256,1024]{1,0:T(8,128)(2,1)S(1)}, u32[]{:S(2)}, u32[]{:S(2)}) collective-permute-start(bf16[256,1024]{1,0:T(8,128)(2,1)S(1)} %pad_maximum_fusion.refs_0_), channel_id=1, source_target_pairs={{2,0},{7,1},{4,2},{1,3},{6,4},{3,5},{0,6},{5,7},{10,8},{15,9},{12,... | collective-permute-start | bytes 1572872 | tf_op jit(solution)/shard_map/ppermute | solution.py:193
  58.2 9.9 %collective-permute-done.3.refs_1_ = bf16[256,1024]{1,0:T(8,128)(2,1)S(1)} collective-permute-done((bf16[256,1024]{1,0:T(8,128)(2,1)S(1)}, bf16[256,1024]{1,0:T(8,128)(2,1)S(1)}, u32[]{:S(2)}, u32[]{:S(2)}) %collective-permute-start.3) | collective-permute-done | bytes 524320 | tf_op jit(solution)/shard_map/ppermute | solution.py:193
  68.1 2.8 %collective-permute-start.5 = (bf16[256,1024]{1,0:T(8,128)(2,1)S(1)}, bf16[256,1024]{1,0:T(8,128)(2,1)S(1)}, u32[]{:S(2)}, u32[]{:S(2)}) collective-permute-start(bf16[256,1024]{1,0:T(8,128)(2,1)S(1)} %collective-permute-done.3.refs_1_), channel_id=1, source_target_pairs={{0,2},{1,7},{2,4},{3,1},{4,6},{5,3},{6,0},{7,5},{8,10},{9,15},{10,... | collective-permute-start | bytes 1572872 | tf_op jit(solution)/shard_map/ppermute | solution.py:194
  70.9 3.9 %shard_map.83 = bf16[16,64,128]{2,1,0:T(8,128)(2,1)} custom-call(bf16[16,192,128]{2,1,0:T(8,128)(2,1)S(1)} %all-to-all-done.x_ref, f32[16,128]{1,0:T(8,128)S(1)} %bitcast.4), custom_call_target="tpu_custom_call" | custom-call | tf_op jit(solution)/shard_map/pallas_call | solution.py:139
  74.8 13.1 %all-to-all-start.1 = ((bf16[16,64,128]{2,1,0:T(8,128)(2,1)}), bf16[16,64,128]{2,1,0:T(8,128)(2,1)S(1)}, u32[]{:S(2)}, u32[]{:S(2)}) async-start(bf16[16,64,128]{2,1,0:T(8,128)(2,1)} %shard_map.83), calls=%async_computation.1 | async-start | bytes 524288 | tf_op jit(solution)/shard_map/all_to_all | solution.py:209
  87.9 1.9 %collective-permute-start.6 = (bf16[256,1024]{1,0:T(8,128)(2,1)S(1)}, bf16[256,1024]{1,0:T(8,128)(2,1)S(1)}, u32[]{:S(2)}, u32[]{:S(2)}) collective-permute-start(bf16[256,1024]{1,0:T(8,128)(2,1)S(1)} %pad_maximum_fusion.refs_0_), channel_id=1, source_target_pairs={{0,1},{1,0},{2,3},{3,2},{4,5},{5,4},{6,7},{7,6},{8,9},{9,8},{10,11... | collective-permute-start | bytes 1572872 | tf_op jit(solution)/shard_map/ppermute | solution.py:183
  89.8 2.4 %collective-permute-start.7 = (bf16[256,1024]{1,0:T(8,128)(2,1)S(1)}, bf16[256,1024]{1,0:T(8,128)(2,1)S(1)}, u32[]{:S(2)}, u32[]{:S(2)}) collective-permute-start(bf16[256,1024]{1,0:T(8,128)(2,1)S(1)} %collective-permute-done.3.refs_1_), channel_id=1, source_target_pairs={{0,1},{1,0},{2,3},{3,2},{4,5},{5,4},{6,7},{7,6},{8,9},{9,8},{10,11... | collective-permute-start | bytes 1572872 | tf_op jit(solution)/shard_map/ppermute | solution.py:183
  92.3 1.9 %collective-permute-start.8 = (bf16[256,1024]{1,0:T(8,128)(2,1)S(1)}, bf16[256,1024]{1,0:T(8,128)(2,1)}, u32[]{:S(2)}, u32[]{:S(2)}) collective-permute-start(bf16[256,1024]{1,0:T(8,128)(2,1)S(1)} %collective-permute-done.4.refs_2_), channel_id=1, source_target_pairs={{0,1},{1,0},{2,3},{3,2},{4,5},{5,4},{6,7},{7,6},{8,9},{9,8},{10,11... | collective-permute-start | bytes 1572872 | tf_op jit(solution)/shard_map/ppermute | solution.py:183
  94.2 2.4 %collective-permute-start.9 = (bf16[256,1024]{1,0:T(8,128)(2,1)S(1)}, bf16[256,1024]{1,0:T(8,128)(2,1)}, u32[]{:S(2)}, u32[]{:S(2)}) collective-permute-start(bf16[256,1024]{1,0:T(8,128)(2,1)S(1)} %collective-permute-done.5.refs_3_), channel_id=1, source_target_pairs={{0,1},{1,0},{2,3},{3,2},{4,5},{5,4},{6,7},{7,6},{8,9},{9,8},{10,11... | collective-permute-start | bytes 1572872 | tf_op jit(solution)/shard_map/ppermute | solution.py:183
  96.7 0.6 copy-done.2
  97.3 0.0 copy-done.4
  97.3 0.1 pad_add_fusion.base_ref
  97.4 0.8 collective-permute-done.9.refs_7_
  98.3 6.1 %all-to-all-done.1 = bf16[16,64,128]{2,1,0:T(8,128)(2,1)S(1)} async-done(((bf16[16,64,128]{2,1,0:T(8,128)(2,1)}), bf16[16,64,128]{2,1,0:T(8,128)(2,1)S(1)}, u32[]{:S(2)}, u32[]{:S(2)}) %all-to-all-start.1) | async-done | bytes 262176 | tf_op jit(solution)/shard_map/all_to_all | solution.py:209
  104.4 3.4 %shard_map.84 = bf16[1,128,2048]{2,1,0:T(8,128)(2,1)} custom-call(s32[16]{0:T(128)S(1)} %pad_add_fusion.base_ref, bf16[1024,128]{1,0:T(8,128)(2,1)S(1)} %bitcast.3, bf16[256,1024]{1,0:T(8,128)(2,1)S(1)} %pad_maximum_fusion.refs_0_, bf16[256,1024]{1,0:T(8,128)(2,1)S(1)} %collective-permute-done.3.refs_1_, ...), custom_call_target="tpu_custom_call" | custom-call | tf_op jit(solution)/shard_map/pallas_call | solution.py:171
  (18 shorter events, 0.1 us)
Async XLA Ops:
  2.1 19.0 %copy-start.1 = (bf16[1024,32]{0,1:T(8,128)(2,1)S(1)}, bf16[1024,32]{0,1:T(8,128)(2,1)}, u32[]{:S(2)}) copy-start(bf16[1024,32]{0,1:T(8,128)(2,1)} %param.12) | copy-start | bytes 196612
  2.1 68.8 %all-to-all-start = ((bf16[16,192,128]{2,1,0:T(8,128)(2,1)}), bf16[16,192,128]{2,1,0:T(8,128)(2,1)S(1)}, u32[]{:S(2)}, u32[]{:S(2)}) async-start(bf16[16,192,128]{2,1,0:T(8,128)(2,1)} %shard_map.82), calls=%async_computation | async-start | bytes 1572864 | tf_op jit(solution)/shard_map/all_to_all | solution.py:206
  21.2 10.8 %collective-permute-start = (bf16[32,1024]{1,0:T(8,128)(2,1)S(1)}, bf16[32,1024]{1,0:T(8,128)(2,1)S(1)}, u32[]{:S(2)}, u32[]{:S(2)}) collective-permute-start(bf16[32,1024]{1,0:T(8,128)(2,1)S(1)} %bitcast.5), channel_id=1, source_target_pairs={{0,32},{8,40},{16,48},{24,56},{32,0},{40,8},{48,16},{56,24},{1,33}... | collective-permute-start | bytes 196616 | tf_op jit(solution)/shard_map/ppermute | solution.py:183
  32.0 9.3 %collective-permute-start.1 = (bf16[64,1024]{1,0:T(8,128)(2,1)S(1)}, bf16[64,1024]{1,0:T(8,128)(2,1)S(1)}, u32[]{:S(2)}, u32[]{:S(2)}) collective-permute-start(bf16[64,1024]{1,0:T(8,128)(2,1)S(1)} %pad_maximum_fusion.2), channel_id=1, source_target_pairs={{0,16},{8,24},{16,32},{24,40},{32,48},{40,56},{48,0},{56,8},{1,17}... | collective-permute-start | bytes 393224 | tf_op jit(solution)/shard_map/ppermute | solution.py:183
  41.4 29.5 %copy-start = (f32[1,1,2048]{2,1,0:T(1,128)S(1)}, f32[1,1,2048]{2,1,0:T(1,128)}, u32[]{:S(2)}) copy-start(f32[1,1,2048]{2,1,0:T(1,128)} %param.11) | copy-start | bytes 24580
  41.4 9.7 %collective-permute-start.2 = (bf16[128,1024]{1,0:T(8,128)(2,1)S(1)}, bf16[128,1024]{1,0:T(8,128)(2,1)S(1)}, u32[]{:S(2)}, u32[]{:S(2)}) collective-permute-start(bf16[128,1024]{1,0:T(8,128)(2,1)S(1)} %pad_maximum_fusion.1), channel_id=1, source_target_pairs={{0,8},{8,16},{16,24},{24,32},{32,40},{40,48},{48,56},{56,0},{1,9},... | collective-permute-start | bytes 786440 | tf_op jit(solution)/shard_map/ppermute | solution.py:183
  51.1 17.0 %collective-permute-start.3 = (bf16[256,1024]{1,0:T(8,128)(2,1)S(1)}, bf16[256,1024]{1,0:T(8,128)(2,1)S(1)}, u32[]{:S(2)}, u32[]{:S(2)}) collective-permute-start(bf16[256,1024]{1,0:T(8,128)(2,1)S(1)} %pad_maximum_fusion.refs_0_), channel_id=1, source_target_pairs={{0,2},{1,7},{2,4},{3,1},{4,6},{5,3},{6,0},{7,5},{8,10},{9,15},{10,... | collective-permute-start | bytes 1572872 | tf_op jit(solution)/shard_map/ppermute | solution.py:193
  54.5 37.8 %collective-permute-start.4 = (bf16[256,1024]{1,0:T(8,128)(2,1)S(1)}, bf16[256,1024]{1,0:T(8,128)(2,1)S(1)}, u32[]{:S(2)}, u32[]{:S(2)}) collective-permute-start(bf16[256,1024]{1,0:T(8,128)(2,1)S(1)} %pad_maximum_fusion.refs_0_), channel_id=1, source_target_pairs={{2,0},{7,1},{4,2},{1,3},{6,4},{3,5},{0,6},{5,7},{10,8},{15,9},{12,... | collective-permute-start | bytes 1572872 | tf_op jit(solution)/shard_map/ppermute | solution.py:193
  68.1 26.1 %collective-permute-start.5 = (bf16[256,1024]{1,0:T(8,128)(2,1)S(1)}, bf16[256,1024]{1,0:T(8,128)(2,1)S(1)}, u32[]{:S(2)}, u32[]{:S(2)}) collective-permute-start(bf16[256,1024]{1,0:T(8,128)(2,1)S(1)} %collective-permute-done.3.refs_1_), channel_id=1, source_target_pairs={{0,2},{1,7},{2,4},{3,1},{4,6},{5,3},{6,0},{7,5},{8,10},{9,15},{10,... | collective-permute-start | bytes 1572872 | tf_op jit(solution)/shard_map/ppermute | solution.py:194
  74.8 29.6 %all-to-all-start.1 = ((bf16[16,64,128]{2,1,0:T(8,128)(2,1)}), bf16[16,64,128]{2,1,0:T(8,128)(2,1)S(1)}, u32[]{:S(2)}, u32[]{:S(2)}) async-start(bf16[16,64,128]{2,1,0:T(8,128)(2,1)} %shard_map.83), calls=%async_computation.1 | async-start | bytes 524288 | tf_op jit(solution)/shard_map/all_to_all | solution.py:209
  87.9 9.5 %collective-permute-start.6 = (bf16[256,1024]{1,0:T(8,128)(2,1)S(1)}, bf16[256,1024]{1,0:T(8,128)(2,1)S(1)}, u32[]{:S(2)}, u32[]{:S(2)}) collective-permute-start(bf16[256,1024]{1,0:T(8,128)(2,1)S(1)} %pad_maximum_fusion.refs_0_), channel_id=1, source_target_pairs={{0,1},{1,0},{2,3},{3,2},{4,5},{5,4},{6,7},{7,6},{8,9},{9,8},{10,11... | collective-permute-start | bytes 1572872 | tf_op jit(solution)/shard_map/ppermute | solution.py:183
  89.8 7.6 %collective-permute-start.7 = (bf16[256,1024]{1,0:T(8,128)(2,1)S(1)}, bf16[256,1024]{1,0:T(8,128)(2,1)S(1)}, u32[]{:S(2)}, u32[]{:S(2)}) collective-permute-start(bf16[256,1024]{1,0:T(8,128)(2,1)S(1)} %collective-permute-done.3.refs_1_), channel_id=1, source_target_pairs={{0,1},{1,0},{2,3},{3,2},{4,5},{5,4},{6,7},{7,6},{8,9},{9,8},{10,11... | collective-permute-start | bytes 1572872 | tf_op jit(solution)/shard_map/ppermute | solution.py:183
  92.3 5.2 %collective-permute-start.8 = (bf16[256,1024]{1,0:T(8,128)(2,1)S(1)}, bf16[256,1024]{1,0:T(8,128)(2,1)}, u32[]{:S(2)}, u32[]{:S(2)}) collective-permute-start(bf16[256,1024]{1,0:T(8,128)(2,1)S(1)} %collective-permute-done.4.refs_2_), channel_id=1, source_target_pairs={{0,1},{1,0},{2,3},{3,2},{4,5},{5,4},{6,7},{7,6},{8,9},{9,8},{10,11... | collective-permute-start | bytes 1572872 | tf_op jit(solution)/shard_map/ppermute | solution.py:183
  94.2 4.1 %collective-permute-start.9 = (bf16[256,1024]{1,0:T(8,128)(2,1)S(1)}, bf16[256,1024]{1,0:T(8,128)(2,1)}, u32[]{:S(2)}, u32[]{:S(2)}) collective-permute-start(bf16[256,1024]{1,0:T(8,128)(2,1)S(1)} %collective-permute-done.5.refs_3_), channel_id=1, source_target_pairs={{0,1},{1,0},{2,3},{3,2},{4,5},{5,4},{6,7},{7,6},{8,9},{9,8},{10,11... | collective-permute-start | bytes 1572872 | tf_op jit(solution)/shard_map/ppermute | solution.py:183
  96.6 0.7 copy-start.2
  96.6 0.7 copy-start.3
  96.7 0.7 copy-start.4

commit v3 on v2

--- a/solution.py
+++ b/solution.py
@@ -9,7 +9,6 @@
 
 DP = ("dp_0", "dp_1", "dp_2")
 VMEM = pl.BlockSpec(memory_space=pltpu.VMEM)
-SMEM = pl.BlockSpec(memory_space=pltpu.SMEM)
 HBM = pl.BlockSpec(memory_space=pltpu.HBM)
 STEP, PART = 256, 128
 
@@ -154,28 +153,32 @@
     )(packed, cum)
 
 
-def project_kernel(base_ref, head_ref, *refs):
+def project_kernel(spot_ref, head_ref, *refs):
     *parts, out_ref, turned_ref = refs
+    y, x, core = spot_ref[0], spot_ref[1], spot_ref[2]
     heads = head_ref[...]
     for n, part in enumerate(parts):
+        owner = core if n < 4 else 1 - core
+        base = (((x + (0, -1, 1, 2)[n % 4] * (1 - 2 * owner)) & 3) * 2 + owner) * 32
         rows = jnp.dot(part[...], heads, preferred_element_type=jnp.float32)
-        for y in range(8):
-            place = pl.multiple_of(base_ref[n] + base_ref[len(parts) + y], 32)
-            turned_ref[pl.ds(place, 32), :] = rows[y * 32 : (y + 1) * 32]
+        for m, back in enumerate((0, 4, 2, 6, 1, 5, 3, 7)):
+            place = pl.multiple_of(((y - back) & 7) * 256 + base, 32)
+            turned_ref[pl.ds(place, 32), :] = rows[m * 32 : (m + 1) * 32]
     for n in range(out_ref.shape[2] // 128):
         cols = slice(n * 128, (n + 1) * 128)
         out_ref[0, :, cols] = turned_ref[cols, :].astype(jnp.bfloat16).T
 
 
-def project(heads, parts, bases):
+def project(heads, parts):
+    spot = jnp.stack([lax.axis_index(axis) for axis in DP])
     return pl.pallas_call(
         project_kernel,
         out_shape=jax.ShapeDtypeStruct((1, 128, 2048), jnp.bfloat16),
-        in_specs=[SMEM] + [VMEM] * 9,
+        in_specs=[pl.BlockSpec(memory_space=pltpu.SMEM)] + [VMEM] * (1 + len(parts)),
         out_specs=VMEM,
         scratch_shapes=[pltpu.VMEM((2048, 128), jnp.float32)],
         compiler_params=pltpu.CompilerParams(vmem_limit_bytes=12 << 20),
-    )(bases, heads, *parts)
+    )(spot, heads, *parts)
 
 
 def shift(value, axis, by):
@@ -184,7 +187,6 @@
 
 
 def gather_weight(out_weight):
-    y, x, core = (lax.axis_index(axis) for axis in DP)
     rows = out_weight.T
     for by in (4, 2, 1):
         rows = jnp.concatenate([rows, shift(rows, "dp_0", by)])
@@ -195,19 +197,16 @@
     pieces = [rows, *near, far]
     others = [shift(rows, "dp_2", 1)]
     others += [shift(piece, "dp_2", 1) for piece in pieces[1:]]
-    cores = core ^ jnp.array([0, 0, 0, 0, 1, 1, 1, 1], jnp.int32)
-    owners = (x + jnp.array([0, -1, 1, 2] * 2, jnp.int32) * (1 - 2 * cores)) & 3
-    places = (y - jnp.array([0, 4, 2, 6, 1, 5, 3, 7], jnp.int32)) & 7
-    return pieces + others, jnp.concatenate([(owners * 2 + cores) * 32, places * 256])
+    return pieces + others
 
 
 def shards(queries, keys, values, cum_gates, out_weight):
     packed = pack(queries, keys, values)
     packed = lax.all_to_all(packed, "sp", split_axis=0, concat_axis=0, tiled=True)
-    parts, bases = gather_weight(out_weight)
+    parts = gather_weight(out_weight)
     heads = attend(packed, cum_gates.reshape(16, 128))
     heads = lax.all_to_all(heads, "sp", split_axis=0, concat_axis=0, tiled=True)
-    return project(heads.reshape(1024, 128), parts, bases)
+    return project(heads.reshape(1024, 128), parts)
 
 
 def solution(mesh):

time: 108 us -> 108 us (level)
  no operation moved by 1% of the time
where the time goes in v3:
time: 108 us
  starting transfers between devices  58.9 us (55%)
  waiting for transfers between devices  39.1 us (36%)
  Pallas kernels  9.45 us (9%)
    ppermute x7, waiting for transfers between devices, shift(): return lax.ppermute(value, axis, [(s, (s + by) % n) for s in range(n)])  23.1 us
    all_to_all x1, starting transfers between devices, shards(): lax.all_to_all(packed, 'sp', split_axis=0, concat_axis=0, tiled=True)  19 us
    ppermute x7, starting transfers between devices, shift(): return lax.ppermute(value, axis, [(s, (s + by) % n) for s in range(n)])  17 us
    all_to_all x1, starting transfers between devices, shards(): heads = lax.all_to_all(heads, 'sp', split_axis=0, concat_axis=0, tiled=True)  13.1 us
    ppermute x2, waiting for transfers between devices, gather_weight(): near = [lax.ppermute(rows, DP[1:], way) for way in (there, back)]  9.93 us
    ppermute x2, starting transfers between devices, gather_weight(): near = [lax.ppermute(rows, DP[1:], way) for way in (there, back)]  7.05 us
    all_to_all x1, waiting for transfers between devices, shards(): heads = lax.all_to_all(heads, 'sp', split_axis=0, concat_axis=0, tiled=True)  6.08 us
    pallas_call x1, Pallas kernels, attend(): pl.pallas_call(attend_kernel, out_shape=jax.ShapeDtypeStruct((16, 64, 128...  3.91 us
  transfers between devices with their start and end apart: 12, of which 6 were waited for; matrix products, arithmetic and copies ran while one was open for 0% of the time, Pallas kernels for 4%

profile of v3, /device:TPU:32, one launch (start us, length us, event | category | flops | bytes accessed | tf_op | source)
XLA Modules:
  0.0 107.8 jit_solution(1528260256606832197)
XLA Ops:
  0.0 2.1 %shard_map.55 = bf16[16,192,128]{2,1,0:T(8,128)(2,1)} custom-call(bf16[1,128,1024]{2,1,0:T(8,128)(2,1)} %q_hbm.1, bf16[1,128,1024]{2,1,0:T(8,128)(2,1)} %k_hbm.1, bf16[1,128,1024]{2,1,0:T(8,128)(2,1)} %v_hbm.1), custom_call_target="tpu_custom_call" | custom-call | tf_op jit(solution)/shard_map/pallas_call | solution.py:56
  2.1 0.0 copy-start.1
  2.1 19.0 %all-to-all-start = ((bf16[16,192,128]{2,1,0:T(8,128)(2,1)}), bf16[16,192,128]{2,1,0:T(8,128)(2,1)S(1)}, u32[]{:S(2)}, u32[]{:S(2)}) async-start(bf16[16,192,128]{2,1,0:T(8,128)(2,1)} %shard_map.55), calls=%async_computation | async-start | bytes 1572864 | tf_op jit(solution)/shard_map/all_to_all | solution.py:205
  21.2 2.0 %collective-permute-start = (bf16[32,1024]{1,0:T(8,128)(2,1)S(1)}, bf16[32,1024]{1,0:T(8,128)(2,1)S(1)}, u32[]{:S(2)}, u32[]{:S(2)}) collective-permute-start(bf16[32,1024]{1,0:T(8,128)(2,1)S(1)} %bitcast.8), channel_id=1, source_target_pairs={{0,32},{8,40},{16,48},{24,56},{32,0},{40,8},{48,16},{56,24},{1,33}... | collective-permute-start | bytes 196616 | tf_op jit(solution)/shard_map/ppermute | solution.py:186
  23.2 8.8 %collective-permute-done = bf16[32,1024]{1,0:T(8,128)(2,1)S(1)} collective-permute-done((bf16[32,1024]{1,0:T(8,128)(2,1)S(1)}, bf16[32,1024]{1,0:T(8,128)(2,1)S(1)}, u32[]{:S(2)}, u32[]{:S(2)}) %collective-permute-start) | collective-permute-done | bytes 65568 | tf_op jit(solution)/shard_map/ppermute | solution.py:186
  32.0 2.5 %collective-permute-start.1 = (bf16[64,1024]{1,0:T(8,128)(2,1)S(1)}, bf16[64,1024]{1,0:T(8,128)(2,1)S(1)}, u32[]{:S(2)}, u32[]{:S(2)}) collective-permute-start(bf16[64,1024]{1,0:T(8,128)(2,1)S(1)} %pad_maximum_fusion.2), channel_id=1, source_target_pairs={{0,16},{8,24},{16,32},{24,40},{32,48},{40,56},{48,0},{56,8},{1,17}... | collective-permute-start | bytes 393224 | tf_op jit(solution)/shard_map/ppermute | solution.py:186
  34.5 6.9 %collective-permute-done.1 = bf16[64,1024]{1,0:T(8,128)(2,1)S(1)} collective-permute-done((bf16[64,1024]{1,0:T(8,128)(2,1)S(1)}, bf16[64,1024]{1,0:T(8,128)(2,1)S(1)}, u32[]{:S(2)}, u32[]{:S(2)}) %collective-permute-start.1) | collective-permute-done | bytes 131104 | tf_op jit(solution)/shard_map/ppermute | solution.py:186
  41.4 0.0 copy-start
  41.4 3.8 %collective-permute-start.2 = (bf16[128,1024]{1,0:T(8,128)(2,1)S(1)}, bf16[128,1024]{1,0:T(8,128)(2,1)S(1)}, u32[]{:S(2)}, u32[]{:S(2)}) collective-permute-start(bf16[128,1024]{1,0:T(8,128)(2,1)S(1)} %pad_maximum_fusion.1), channel_id=1, source_target_pairs={{0,8},{8,16},{16,24},{24,32},{32,40},{40,48},{48,56},{56,0},{1,9},... | collective-permute-start | bytes 786440 | tf_op jit(solution)/shard_map/ppermute | solution.py:186
  45.2 5.8 %collective-permute-done.2 = bf16[128,1024]{1,0:T(8,128)(2,1)S(1)} collective-permute-done((bf16[128,1024]{1,0:T(8,128)(2,1)S(1)}, bf16[128,1024]{1,0:T(8,128)(2,1)S(1)}, u32[]{:S(2)}, u32[]{:S(2)}) %collective-permute-start.2) | collective-permute-done | bytes 262176 | tf_op jit(solution)/shard_map/ppermute | solution.py:186
  51.1 3.4 %collective-permute-start.3 = (bf16[256,1024]{1,0:T(8,128)(2,1)S(1)}, bf16[256,1024]{1,0:T(8,128)(2,1)S(1)}, u32[]{:S(2)}, u32[]{:S(2)}) collective-permute-start(bf16[256,1024]{1,0:T(8,128)(2,1)S(1)} %pad_maximum_fusion.refs_0_), channel_id=1, source_target_pairs={{0,2},{1,7},{2,4},{3,1},{4,6},{5,3},{6,0},{7,5},{8,10},{9,15},{10,... | collective-permute-start | bytes 1572872 | tf_op jit(solution)/shard_map/ppermute | solution.py:195
  54.5 3.7 %collective-permute-start.4 = (bf16[256,1024]{1,0:T(8,128)(2,1)S(1)}, bf16[256,1024]{1,0:T(8,128)(2,1)S(1)}, u32[]{:S(2)}, u32[]{:S(2)}) collective-permute-start(bf16[256,1024]{1,0:T(8,128)(2,1)S(1)} %pad_maximum_fusion.refs_0_), channel_id=1, source_target_pairs={{2,0},{7,1},{4,2},{1,3},{6,4},{3,5},{0,6},{5,7},{10,8},{15,9},{12,... | collective-permute-start | bytes 1572872 | tf_op jit(solution)/shard_map/ppermute | solution.py:195
  58.2 9.9 %collective-permute-done.3.refs_1_ = bf16[256,1024]{1,0:T(8,128)(2,1)S(1)} collective-permute-done((bf16[256,1024]{1,0:T(8,128)(2,1)S(1)}, bf16[256,1024]{1,0:T(8,128)(2,1)S(1)}, u32[]{:S(2)}, u32[]{:S(2)}) %collective-permute-start.3) | collective-permute-done | bytes 524320 | tf_op jit(solution)/shard_map/ppermute | solution.py:195
  68.1 2.8 %collective-permute-start.5 = (bf16[256,1024]{1,0:T(8,128)(2,1)S(1)}, bf16[256,1024]{1,0:T(8,128)(2,1)S(1)}, u32[]{:S(2)}, u32[]{:S(2)}) collective-permute-start(bf16[256,1024]{1,0:T(8,128)(2,1)S(1)} %collective-permute-done.3.refs_1_), channel_id=1, source_target_pairs={{0,2},{1,7},{2,4},{3,1},{4,6},{5,3},{6,0},{7,5},{8,10},{9,15},{10,... | collective-permute-start | bytes 1572872 | tf_op jit(solution)/shard_map/ppermute | solution.py:196
  70.9 3.9 %shard_map.56 = bf16[16,64,128]{2,1,0:T(8,128)(2,1)} custom-call(bf16[16,192,128]{2,1,0:T(8,128)(2,1)S(1)} %all-to-all-done.x_ref, f32[16,128]{1,0:T(8,128)S(1)} %bitcast.7), custom_call_target="tpu_custom_call" | custom-call | tf_op jit(solution)/shard_map/pallas_call | solution.py:138
  74.8 13.1 %all-to-all-start.1 = ((bf16[16,64,128]{2,1,0:T(8,128)(2,1)}), bf16[16,64,128]{2,1,0:T(8,128)(2,1)S(1)}, u32[]{:S(2)}, u32[]{:S(2)}) async-start(bf16[16,64,128]{2,1,0:T(8,128)(2,1)} %shard_map.56), calls=%async_computation.1 | async-start | bytes 524288 | tf_op jit(solution)/shard_map/all_to_all | solution.py:208
  87.9 1.9 %collective-permute-start.6 = (bf16[256,1024]{1,0:T(8,128)(2,1)S(1)}, bf16[256,1024]{1,0:T(8,128)(2,1)S(1)}, u32[]{:S(2)}, u32[]{:S(2)}) collective-permute-start(bf16[256,1024]{1,0:T(8,128)(2,1)S(1)} %pad_maximum_fusion.refs_0_), channel_id=1, source_target_pairs={{0,1},{1,0},{2,3},{3,2},{4,5},{5,4},{6,7},{7,6},{8,9},{9,8},{10,11... | collective-permute-start | bytes 1572872 | tf_op jit(solution)/shard_map/ppermute | solution.py:186
  89.8 2.4 %collective-permute-start.7 = (bf16[256,1024]{1,0:T(8,128)(2,1)S(1)}, bf16[256,1024]{1,0:T(8,128)(2,1)S(1)}, u32[]{:S(2)}, u32[]{:S(2)}) collective-permute-start(bf16[256,1024]{1,0:T(8,128)(2,1)S(1)} %collective-permute-done.3.refs_1_), channel_id=1, source_target_pairs={{0,1},{1,0},{2,3},{3,2},{4,5},{5,4},{6,7},{7,6},{8,9},{9,8},{10,11... | collective-permute-start | bytes 1572872 | tf_op jit(solution)/shard_map/ppermute | solution.py:186
  92.3 1.9 %collective-permute-start.8 = (bf16[256,1024]{1,0:T(8,128)(2,1)S(1)}, bf16[256,1024]{1,0:T(8,128)(2,1)}, u32[]{:S(2)}, u32[]{:S(2)}) collective-permute-start(bf16[256,1024]{1,0:T(8,128)(2,1)S(1)} %collective-permute-done.4.refs_2_), channel_id=1, source_target_pairs={{0,1},{1,0},{2,3},{3,2},{4,5},{5,4},{6,7},{7,6},{8,9},{9,8},{10,11... | collective-permute-start | bytes 1572872 | tf_op jit(solution)/shard_map/ppermute | solution.py:186
  94.2 2.4 %collective-permute-start.9 = (bf16[256,1024]{1,0:T(8,128)(2,1)S(1)}, bf16[256,1024]{1,0:T(8,128)(2,1)}, u32[]{:S(2)}, u32[]{:S(2)}) collective-permute-start(bf16[256,1024]{1,0:T(8,128)(2,1)S(1)} %collective-permute-done.5.refs_3_), channel_id=1, source_target_pairs={{0,1},{1,0},{2,3},{3,2},{4,5},{5,4},{6,7},{7,6},{8,9},{9,8},{10,11... | collective-permute-start | bytes 1572872 | tf_op jit(solution)/shard_map/ppermute | solution.py:186
  96.6 0.1 pad_add_fusion.spot_ref
  96.7 1.5 %collective-permute-done.9.refs_7_ = bf16[256,1024]{1,0:T(8,128)(2,1)} collective-permute-done((bf16[256,1024]{1,0:T(8,128)(2,1)S(1)}, bf16[256,1024]{1,0:T(8,128)(2,1)}, u32[]{:S(2)}, u32[]{:S(2)}) %collective-permute-start.9) | collective-permute-done | bytes 524320 | tf_op jit(solution)/shard_map/ppermute | solution.py:186
  98.3 6.1 %all-to-all-done.1 = bf16[16,64,128]{2,1,0:T(8,128)(2,1)S(1)} async-done(((bf16[16,64,128]{2,1,0:T(8,128)(2,1)}), bf16[16,64,128]{2,1,0:T(8,128)(2,1)S(1)}, u32[]{:S(2)}, u32[]{:S(2)}) %all-to-all-start.1) | async-done | bytes 262176 | tf_op jit(solution)/shard_map/all_to_all | solution.py:208
  104.4 3.4 %shard_map.57 = bf16[1,128,2048]{2,1,0:T(8,128)(2,1)} custom-call(s32[3]{0:T(128)S(1)} %pad_add_fusion.spot_ref, bf16[1024,128]{1,0:T(8,128)(2,1)S(1)} %bitcast.6, bf16[256,1024]{1,0:T(8,128)(2,1)S(1)} %pad_maximum_fusion.refs_0_, bf16[256,1024]{1,0:T(8,128)(2,1)S(1)} %collective-permute-done.3.refs_1_, ...), custom_call_target="tpu_custom_call" | custom-call | tf_op jit(solution)/shard_map/pallas_call | solution.py:174
  (11 shorter events, 0.1 us)
Async XLA Ops:
  2.1 19.0 %copy-start.1 = (bf16[1024,32]{0,1:T(8,128)(2,1)S(1)}, bf16[1024,32]{0,1:T(8,128)(2,1)}, u32[]{:S(2)}) copy-start(bf16[1024,32]{0,1:T(8,128)(2,1)} %param.9) | copy-start | bytes 196612
  2.1 68.8 %all-to-all-start = ((bf16[16,192,128]{2,1,0:T(8,128)(2,1)}), bf16[16,192,128]{2,1,0:T(8,128)(2,1)S(1)}, u32[]{:S(2)}, u32[]{:S(2)}) async-start(bf16[16,192,128]{2,1,0:T(8,128)(2,1)} %shard_map.55), calls=%async_computation | async-start | bytes 1572864 | tf_op jit(solution)/shard_map/all_to_all | solution.py:205
  21.2 10.8 %collective-permute-start = (bf16[32,1024]{1,0:T(8,128)(2,1)S(1)}, bf16[32,1024]{1,0:T(8,128)(2,1)S(1)}, u32[]{:S(2)}, u32[]{:S(2)}) collective-permute-start(bf16[32,1024]{1,0:T(8,128)(2,1)S(1)} %bitcast.8), channel_id=1, source_target_pairs={{0,32},{8,40},{16,48},{24,56},{32,0},{40,8},{48,16},{56,24},{1,33}... | collective-permute-start | bytes 196616 | tf_op jit(solution)/shard_map/ppermute | solution.py:186
  32.0 9.3 %collective-permute-start.1 = (bf16[64,1024]{1,0:T(8,128)(2,1)S(1)}, bf16[64,1024]{1,0:T(8,128)(2,1)S(1)}, u32[]{:S(2)}, u32[]{:S(2)}) collective-permute-start(bf16[64,1024]{1,0:T(8,128)(2,1)S(1)} %pad_maximum_fusion.2), channel_id=1, source_target_pairs={{0,16},{8,24},{16,32},{24,40},{32,48},{40,56},{48,0},{56,8},{1,17}... | collective-permute-start | bytes 393224 | tf_op jit(solution)/shard_map/ppermute | solution.py:186
  41.4 29.5 %copy-start = (f32[1,1,2048]{2,1,0:T(1,128)S(1)}, f32[1,1,2048]{2,1,0:T(1,128)}, u32[]{:S(2)}) copy-start(f32[1,1,2048]{2,1,0:T(1,128)} %param.8) | copy-start | bytes 24580
  41.4 9.7 %collective-permute-start.2 = (bf16[128,1024]{1,0:T(8,128)(2,1)S(1)}, bf16[128,1024]{1,0:T(8,128)(2,1)S(1)}, u32[]{:S(2)}, u32[]{:S(2)}) collective-permute-start(bf16[128,1024]{1,0:T(8,128)(2,1)S(1)} %pad_maximum_fusion.1), channel_id=1, source_target_pairs={{0,8},{8,16},{16,24},{24,32},{32,40},{40,48},{48,56},{56,0},{1,9},... | collective-permute-start | bytes 786440 | tf_op jit(solution)/shard_map/ppermute | solution.py:186
  51.1 17.0 %collective-permute-start.3 = (bf16[256,1024]{1,0:T(8,128)(2,1)S(1)}, bf16[256,1024]{1,0:T(8,128)(2,1)S(1)}, u32[]{:S(2)}, u32[]{:S(2)}) collective-permute-start(bf16[256,1024]{1,0:T(8,128)(2,1)S(1)} %pad_maximum_fusion.refs_0_), channel_id=1, source_target_pairs={{0,2},{1,7},{2,4},{3,1},{4,6},{5,3},{6,0},{7,5},{8,10},{9,15},{10,... | collective-permute-start | bytes 1572872 | tf_op jit(solution)/shard_map/ppermute | solution.py:195
  54.5 37.8 %collective-permute-start.4 = (bf16[256,1024]{1,0:T(8,128)(2,1)S(1)}, bf16[256,1024]{1,0:T(8,128)(2,1)S(1)}, u32[]{:S(2)}, u32[]{:S(2)}) collective-permute-start(bf16[256,1024]{1,0:T(8,128)(2,1)S(1)} %pad_maximum_fusion.refs_0_), channel_id=1, source_target_pairs={{2,0},{7,1},{4,2},{1,3},{6,4},{3,5},{0,6},{5,7},{10,8},{15,9},{12,... | collective-permute-start | bytes 1572872 | tf_op jit(solution)/shard_map/ppermute | solution.py:195
  68.1 26.1 %collective-permute-start.5 = (bf16[256,1024]{1,0:T(8,128)(2,1)S(1)}, bf16[256,1024]{1,0:T(8,128)(2,1)S(1)}, u32[]{:S(2)}, u32[]{:S(2)}) collective-permute-start(bf16[256,1024]{1,0:T(8,128)(2,1)S(1)} %collective-permute-done.3.refs_1_), channel_id=1, source_target_pairs={{0,2},{1,7},{2,4},{3,1},{4,6},{5,3},{6,0},{7,5},{8,10},{9,15},{10,... | collective-permute-start | bytes 1572872 | tf_op jit(solution)/shard_map/ppermute | solution.py:196
  74.8 29.5 %all-to-all-start.1 = ((bf16[16,64,128]{2,1,0:T(8,128)(2,1)}), bf16[16,64,128]{2,1,0:T(8,128)(2,1)S(1)}, u32[]{:S(2)}, u32[]{:S(2)}) async-start(bf16[16,64,128]{2,1,0:T(8,128)(2,1)} %shard_map.56), calls=%async_computation.1 | async-start | bytes 524288 | tf_op jit(solution)/shard_map/all_to_all | solution.py:208
  87.9 8.8 %collective-permute-start.6 = (bf16[256,1024]{1,0:T(8,128)(2,1)S(1)}, bf16[256,1024]{1,0:T(8,128)(2,1)S(1)}, u32[]{:S(2)}, u32[]{:S(2)}) collective-permute-start(bf16[256,1024]{1,0:T(8,128)(2,1)S(1)} %pad_maximum_fusion.refs_0_), channel_id=1, source_target_pairs={{0,1},{1,0},{2,3},{3,2},{4,5},{5,4},{6,7},{7,6},{8,9},{9,8},{10,11... | collective-permute-start | bytes 1572872 | tf_op jit(solution)/shard_map/ppermute | solution.py:186
  89.8 6.9 %collective-permute-start.7 = (bf16[256,1024]{1,0:T(8,128)(2,1)S(1)}, bf16[256,1024]{1,0:T(8,128)(2,1)S(1)}, u32[]{:S(2)}, u32[]{:S(2)}) collective-permute-start(bf16[256,1024]{1,0:T(8,128)(2,1)S(1)} %collective-permute-done.3.refs_1_), channel_id=1, source_target_pairs={{0,1},{1,0},{2,3},{3,2},{4,5},{5,4},{6,7},{7,6},{8,9},{9,8},{10,11... | collective-permute-start | bytes 1572872 | tf_op jit(solution)/shard_map/ppermute | solution.py:186
  92.3 4.4 %collective-permute-start.8 = (bf16[256,1024]{1,0:T(8,128)(2,1)S(1)}, bf16[256,1024]{1,0:T(8,128)(2,1)}, u32[]{:S(2)}, u32[]{:S(2)}) collective-permute-start(bf16[256,1024]{1,0:T(8,128)(2,1)S(1)} %collective-permute-done.4.refs_2_), channel_id=1, source_target_pairs={{0,1},{1,0},{2,3},{3,2},{4,5},{5,4},{6,7},{7,6},{8,9},{9,8},{10,11... | collective-permute-start | bytes 1572872 | tf_op jit(solution)/shard_map/ppermute | solution.py:186
  94.2 4.1 %collective-permute-start.9 = (bf16[256,1024]{1,0:T(8,128)(2,1)S(1)}, bf16[256,1024]{1,0:T(8,128)(2,1)}, u32[]{:S(2)}, u32[]{:S(2)}) collective-permute-start(bf16[256,1024]{1,0:T(8,128)(2,1)S(1)} %collective-permute-done.5.refs_3_), channel_id=1, source_target_pairs={{0,1},{1,0},{2,3},{3,2},{4,5},{5,4},{6,7},{7,6},{8,9},{9,8},{10,11... | collective-permute-start | bytes 1572872 | tf_op jit(solution)/shard_map/ppermute | solution.py:186

commit v4 on v3

--- a/solution.py
+++ b/solution.py
@@ -121,14 +121,15 @@
         late = list(range(0, (before + 1) * STEP, PART)) if n else []
         top = None
         for m in range(max(len(todo), len(late))):
+            if m == min(2, max(len(todo), len(late)) - 1) and n > 1:
+                finish(order[n - 2])
             if m < len(late):
                 weigh(before, late[m], tops[before])
             if m < len(todo):
                 top = score(i, todo[m], top)
         if top is not None:
             tops[i] = jnp.max(top, axis=0, keepdims=True)
-        if n:
-            finish(before)
+    finish(order[-1])
     for copy in copies:
         copy.wait()
 
@@ -154,7 +155,7 @@
 
 
 def project_kernel(spot_ref, head_ref, *refs):
-    *parts, out_ref, turned_ref = refs
+    *parts, out_hbm, turned_ref, out_ref, sems = refs
     y, x, core = spot_ref[0], spot_ref[1], spot_ref[2]
     heads = head_ref[...]
     for n, part in enumerate(parts):
@@ -164,9 +165,16 @@
         for m, back in enumerate((0, 4, 2, 6, 1, 5, 3, 7)):
             place = pl.multiple_of(((y - back) & 7) * 256 + base, 32)
             turned_ref[pl.ds(place, 32), :] = rows[m * 32 : (m + 1) * 32]
-    for n in range(out_ref.shape[2] // 128):
-        cols = slice(n * 128, (n + 1) * 128)
-        out_ref[0, :, cols] = turned_ref[cols, :].astype(jnp.bfloat16).T
+    copies = []
+    for n in range(4):
+        for m in range(4 * n, 4 * n + 4):
+            cols = slice(m * 128, (m + 1) * 128)
+            out_ref[:, cols] = turned_ref[cols, :].astype(jnp.bfloat16).T
+        cols = slice(n * 512, (n + 1) * 512)
+        copies.append(pltpu.make_async_copy(out_ref.at[:, cols], out_hbm.at[0, :, cols], sems.at[n]))
+        copies[-1].start()
+    for copy in copies:
+        copy.wait()
 
 
 def project(heads, parts):
@@ -175,8 +183,12 @@
         project_kernel,
         out_shape=jax.ShapeDtypeStruct((1, 128, 2048), jnp.bfloat16),
         in_specs=[pl.BlockSpec(memory_space=pltpu.SMEM)] + [VMEM] * (1 + len(parts)),
-        out_specs=VMEM,
-        scratch_shapes=[pltpu.VMEM((2048, 128), jnp.float32)],
+        out_specs=HBM,
+        scratch_shapes=[
+            pltpu.VMEM((2048, 128), jnp.float32),
+            pltpu.VMEM((128, 2048), jnp.bfloat16),
+            pltpu.SemaphoreType.DMA((4,)),
+        ],
         compiler_params=pltpu.CompilerParams(vmem_limit_bytes=12 << 20),
     )(spot, heads, *parts)
 

time: 108 us -> 108 us (level)
  no operation moved by 1% of the time
where the time goes in v4:
time: 108 us
  starting transfers between devices  58.9 us (55%)
  waiting for transfers between devices  39.1 us (36%)
  Pallas kernels  9.31 us (9%)
    ppermute x7, waiting for transfers between devices, shift(): return lax.ppermute(value, axis, [(s, (s + by) % n) for s in range(n)])  23.1 us
    all_to_all x1, starting transfers between devices, shards(): lax.all_to_all(packed, 'sp', split_axis=0, concat_axis=0, tiled=True)  19 us
    ppermute x7, starting transfers between devices, shift(): return lax.ppermute(value, axis, [(s, (s + by) % n) for s in range(n)])  17 us
    all_to_all x1, starting transfers between devices, shards(): heads = lax.all_to_all(heads, 'sp', split_axis=0, concat_axis=0, tiled=True)  13.1 us
    ppermute x2, waiting for transfers between devices, gather_weight(): near = [lax.ppermute(rows, DP[1:], way) for way in (there, back)]  9.93 us
    ppermute x2, starting transfers between devices, gather_weight(): near = [lax.ppermute(rows, DP[1:], way) for way in (there, back)]  7.05 us
    all_to_all x1, waiting for transfers between devices, shards(): heads = lax.all_to_all(heads, 'sp', split_axis=0, concat_axis=0, tiled=True)  6.1 us
    pallas_call x1, Pallas kernels, attend(): pl.pallas_call(attend_kernel, out_shape=jax.ShapeDtypeStruct((16, 64, 128...  3.84 us
  transfers between devices with their start and end apart: 12, of which 6 were waited for; matrix products, arithmetic and copies ran while one was open for 0% of the time, Pallas kernels for 4%

profile of v4, /device:TPU:32, one launch (start us, length us, event | category | flops | bytes accessed | tf_op | source)
XLA Modules:
  0.0 107.6 jit_solution(15199320829452105036)
XLA Ops:
  0.0 2.1 %shard_map.55 = bf16[16,192,128]{2,1,0:T(8,128)(2,1)} custom-call(bf16[1,128,1024]{2,1,0:T(8,128)(2,1)} %q_hbm.1, bf16[1,128,1024]{2,1,0:T(8,128)(2,1)} %k_hbm.1, bf16[1,128,1024]{2,1,0:T(8,128)(2,1)} %v_hbm.1), custom_call_target="tpu_custom_call" | custom-call | tf_op jit(solution)/shard_map/pallas_call | solution.py:56
  2.1 0.0 copy-start.1
  2.1 19.0 %all-to-all-start = ((bf16[16,192,128]{2,1,0:T(8,128)(2,1)}), bf16[16,192,128]{2,1,0:T(8,128)(2,1)S(1)}, u32[]{:S(2)}, u32[]{:S(2)}) async-start(bf16[16,192,128]{2,1,0:T(8,128)(2,1)} %shard_map.55), calls=%async_computation | async-start | bytes 1572864 | tf_op jit(solution)/shard_map/all_to_all | solution.py:217
  21.2 2.0 %collective-permute-start = (bf16[32,1024]{1,0:T(8,128)(2,1)S(1)}, bf16[32,1024]{1,0:T(8,128)(2,1)S(1)}, u32[]{:S(2)}, u32[]{:S(2)}) collective-permute-start(bf16[32,1024]{1,0:T(8,128)(2,1)S(1)} %bitcast.8), channel_id=1, source_target_pairs={{0,32},{8,40},{16,48},{24,56},{32,0},{40,8},{48,16},{56,24},{1,33}... | collective-permute-start | bytes 196616 | tf_op jit(solution)/shard_map/ppermute | solution.py:198
  23.2 8.8 %collective-permute-done = bf16[32,1024]{1,0:T(8,128)(2,1)S(1)} collective-permute-done((bf16[32,1024]{1,0:T(8,128)(2,1)S(1)}, bf16[32,1024]{1,0:T(8,128)(2,1)S(1)}, u32[]{:S(2)}, u32[]{:S(2)}) %collective-permute-start) | collective-permute-done | bytes 65568 | tf_op jit(solution)/shard_map/ppermute | solution.py:198
  32.0 2.5 %collective-permute-start.1 = (bf16[64,1024]{1,0:T(8,128)(2,1)S(1)}, bf16[64,1024]{1,0:T(8,128)(2,1)S(1)}, u32[]{:S(2)}, u32[]{:S(2)}) collective-permute-start(bf16[64,1024]{1,0:T(8,128)(2,1)S(1)} %pad_maximum_fusion.2), channel_id=1, source_target_pairs={{0,16},{8,24},{16,32},{24,40},{32,48},{40,56},{48,0},{56,8},{1,17}... | collective-permute-start | bytes 393224 | tf_op jit(solution)/shard_map/ppermute | solution.py:198
  34.5 6.9 %collective-permute-done.1 = bf16[64,1024]{1,0:T(8,128)(2,1)S(1)} collective-permute-done((bf16[64,1024]{1,0:T(8,128)(2,1)S(1)}, bf16[64,1024]{1,0:T(8,128)(2,1)S(1)}, u32[]{:S(2)}, u32[]{:S(2)}) %collective-permute-start.1) | collective-permute-done | bytes 131104 | tf_op jit(solution)/shard_map/ppermute | solution.py:198
  41.4 0.0 copy-start
  41.4 3.8 %collective-permute-start.2 = (bf16[128,1024]{1,0:T(8,128)(2,1)S(1)}, bf16[128,1024]{1,0:T(8,128)(2,1)S(1)}, u32[]{:S(2)}, u32[]{:S(2)}) collective-permute-start(bf16[128,1024]{1,0:T(8,128)(2,1)S(1)} %pad_maximum_fusion.1), channel_id=1, source_target_pairs={{0,8},{8,16},{16,24},{24,32},{32,40},{40,48},{48,56},{56,0},{1,9},... | collective-permute-start | bytes 786440 | tf_op jit(solution)/shard_map/ppermute | solution.py:198
  45.2 5.8 %collective-permute-done.2 = bf16[128,1024]{1,0:T(8,128)(2,1)S(1)} collective-permute-done((bf16[128,1024]{1,0:T(8,128)(2,1)S(1)}, bf16[128,1024]{1,0:T(8,128)(2,1)S(1)}, u32[]{:S(2)}, u32[]{:S(2)}) %collective-permute-start.2) | collective-permute-done | bytes 262176 | tf_op jit(solution)/shard_map/ppermute | solution.py:198
  51.1 3.4 %collective-permute-start.3 = (bf16[256,1024]{1,0:T(8,128)(2,1)S(1)}, bf16[256,1024]{1,0:T(8,128)(2,1)S(1)}, u32[]{:S(2)}, u32[]{:S(2)}) collective-permute-start(bf16[256,1024]{1,0:T(8,128)(2,1)S(1)} %pad_maximum_fusion.refs_0_), channel_id=1, source_target_pairs={{0,2},{1,7},{2,4},{3,1},{4,6},{5,3},{6,0},{7,5},{8,10},{9,15},{10,... | collective-permute-start | bytes 1572872 | tf_op jit(solution)/shard_map/ppermute | solution.py:207
  54.5 3.7 %collective-permute-start.4 = (bf16[256,1024]{1,0:T(8,128)(2,1)S(1)}, bf16[256,1024]{1,0:T(8,128)(2,1)S(1)}, u32[]{:S(2)}, u32[]{:S(2)}) collective-permute-start(bf16[256,1024]{1,0:T(8,128)(2,1)S(1)} %pad_maximum_fusion.refs_0_), channel_id=1, source_target_pairs={{2,0},{7,1},{4,2},{1,3},{6,4},{3,5},{0,6},{5,7},{10,8},{15,9},{12,... | collective-permute-start | bytes 1572872 | tf_op jit(solution)/shard_map/ppermute | solution.py:207
  58.2 9.9 %collective-permute-done.3.refs_1_ = bf16[256,1024]{1,0:T(8,128)(2,1)S(1)} collective-permute-done((bf16[256,1024]{1,0:T(8,128)(2,1)S(1)}, bf16[256,1024]{1,0:T(8,128)(2,1)S(1)}, u32[]{:S(2)}, u32[]{:S(2)}) %collective-permute-start.3) | collective-permute-done | bytes 524320 | tf_op jit(solution)/shard_map/ppermute | solution.py:207
  68.1 2.8 %collective-permute-start.5 = (bf16[256,1024]{1,0:T(8,128)(2,1)S(1)}, bf16[256,1024]{1,0:T(8,128)(2,1)S(1)}, u32[]{:S(2)}, u32[]{:S(2)}) collective-permute-start(bf16[256,1024]{1,0:T(8,128)(2,1)S(1)} %collective-permute-done.3.refs_1_), channel_id=1, source_target_pairs={{0,2},{1,7},{2,4},{3,1},{4,6},{5,3},{6,0},{7,5},{8,10},{9,15},{10,... | collective-permute-start | bytes 1572872 | tf_op jit(solution)/shard_map/ppermute | solution.py:208
  70.9 3.8 %shard_map.56 = bf16[16,64,128]{2,1,0:T(8,128)(2,1)} custom-call(bf16[16,192,128]{2,1,0:T(8,128)(2,1)S(1)} %all-to-all-done.x_ref, f32[16,128]{1,0:T(8,128)S(1)} %bitcast.7), custom_call_target="tpu_custom_call" | custom-call | tf_op jit(solution)/shard_map/pallas_call | solution.py:139
  74.8 13.1 %all-to-all-start.1 = ((bf16[16,64,128]{2,1,0:T(8,128)(2,1)}), bf16[16,64,128]{2,1,0:T(8,128)(2,1)S(1)}, u32[]{:S(2)}, u32[]{:S(2)}) async-start(bf16[16,64,128]{2,1,0:T(8,128)(2,1)} %shard_map.56), calls=%async_computation.1 | async-start | bytes 524288 | tf_op jit(solution)/shard_map/all_to_all | solution.py:220
  87.8 1.9 %collective-permute-start.6 = (bf16[256,1024]{1,0:T(8,128)(2,1)S(1)}, bf16[256,1024]{1,0:T(8,128)(2,1)S(1)}, u32[]{:S(2)}, u32[]{:S(2)}) collective-permute-start(bf16[256,1024]{1,0:T(8,128)(2,1)S(1)} %pad_maximum_fusion.refs_0_), channel_id=1, source_target_pairs={{0,1},{1,0},{2,3},{3,2},{4,5},{5,4},{6,7},{7,6},{8,9},{9,8},{10,11... | collective-permute-start | bytes 1572872 | tf_op jit(solution)/shard_map/ppermute | solution.py:198
  89.8 2.4 %collective-permute-start.7 = (bf16[256,1024]{1,0:T(8,128)(2,1)S(1)}, bf16[256,1024]{1,0:T(8,128)(2,1)S(1)}, u32[]{:S(2)}, u32[]{:S(2)}) collective-permute-start(bf16[256,1024]{1,0:T(8,128)(2,1)S(1)} %collective-permute-done.3.refs_1_), channel_id=1, source_target_pairs={{0,1},{1,0},{2,3},{3,2},{4,5},{5,4},{6,7},{7,6},{8,9},{9,8},{10,11... | collective-permute-start | bytes 1572872 | tf_op jit(solution)/shard_map/ppermute | solution.py:198
  92.2 1.9 %collective-permute-start.8 = (bf16[256,1024]{1,0:T(8,128)(2,1)S(1)}, bf16[256,1024]{1,0:T(8,128)(2,1)}, u32[]{:S(2)}, u32[]{:S(2)}) collective-permute-start(bf16[256,1024]{1,0:T(8,128)(2,1)S(1)} %collective-permute-done.4.refs_2_), channel_id=1, source_target_pairs={{0,1},{1,0},{2,3},{3,2},{4,5},{5,4},{6,7},{7,6},{8,9},{9,8},{10,11... | collective-permute-start | bytes 1572872 | tf_op jit(solution)/shard_map/ppermute | solution.py:198
  94.1 2.4 %collective-permute-start.9 = (bf16[256,1024]{1,0:T(8,128)(2,1)S(1)}, bf16[256,1024]{1,0:T(8,128)(2,1)}, u32[]{:S(2)}, u32[]{:S(2)}) collective-permute-start(bf16[256,1024]{1,0:T(8,128)(2,1)S(1)} %collective-permute-done.5.refs_3_), channel_id=1, source_target_pairs={{0,1},{1,0},{2,3},{3,2},{4,5},{5,4},{6,7},{7,6},{8,9},{9,8},{10,11... | collective-permute-start | bytes 1572872 | tf_op jit(solution)/shard_map/ppermute | solution.py:198
  96.5 0.1 pad_add_fusion.spot_ref
  96.6 1.5 %collective-permute-done.9.refs_7_ = bf16[256,1024]{1,0:T(8,128)(2,1)} collective-permute-done((bf16[256,1024]{1,0:T(8,128)(2,1)S(1)}, bf16[256,1024]{1,0:T(8,128)(2,1)}, u32[]{:S(2)}, u32[]{:S(2)}) %collective-permute-start.9) | collective-permute-done | bytes 524320 | tf_op jit(solution)/shard_map/ppermute | solution.py:198
  98.2 6.1 %all-to-all-done.1 = bf16[16,64,128]{2,1,0:T(8,128)(2,1)S(1)} async-done(((bf16[16,64,128]{2,1,0:T(8,128)(2,1)}), bf16[16,64,128]{2,1,0:T(8,128)(2,1)S(1)}, u32[]{:S(2)}, u32[]{:S(2)}) %all-to-all-start.1) | async-done | bytes 262176 | tf_op jit(solution)/shard_map/all_to_all | solution.py:220
  104.3 3.4 %shard_map.57 = bf16[1,128,2048]{2,1,0:T(8,128)(2,1)} custom-call(s32[3]{0:T(128)S(1)} %pad_add_fusion.spot_ref, bf16[1024,128]{1,0:T(8,128)(2,1)S(1)} %bitcast.6, bf16[256,1024]{1,0:T(8,128)(2,1)S(1)} %pad_maximum_fusion.refs_0_, bf16[256,1024]{1,0:T(8,128)(2,1)S(1)} %collective-permute-done.3.refs_1_, ...), custom_call_target="tpu_custom_call" | custom-call | tf_op jit(solution)/shard_map/pallas_call | solution.py:182
  (11 shorter events, 0.1 us)
Async XLA Ops:
  2.1 19.0 %copy-start.1 = (bf16[1024,32]{0,1:T(8,128)(2,1)S(1)}, bf16[1024,32]{0,1:T(8,128)(2,1)}, u32[]{:S(2)}) copy-start(bf16[1024,32]{0,1:T(8,128)(2,1)} %param.9) | copy-start | bytes 196612
  2.1 68.8 %all-to-all-start = ((bf16[16,192,128]{2,1,0:T(8,128)(2,1)}), bf16[16,192,128]{2,1,0:T(8,128)(2,1)S(1)}, u32[]{:S(2)}, u32[]{:S(2)}) async-start(bf16[16,192,128]{2,1,0:T(8,128)(2,1)} %shard_map.55), calls=%async_computation | async-start | bytes 1572864 | tf_op jit(solution)/shard_map/all_to_all | solution.py:217
  21.2 10.8 %collective-permute-start = (bf16[32,1024]{1,0:T(8,128)(2,1)S(1)}, bf16[32,1024]{1,0:T(8,128)(2,1)S(1)}, u32[]{:S(2)}, u32[]{:S(2)}) collective-permute-start(bf16[32,1024]{1,0:T(8,128)(2,1)S(1)} %bitcast.8), channel_id=1, source_target_pairs={{0,32},{8,40},{16,48},{24,56},{32,0},{40,8},{48,16},{56,24},{1,33}... | collective-permute-start | bytes 196616 | tf_op jit(solution)/shard_map/ppermute | solution.py:198
  32.0 9.3 %collective-permute-start.1 = (bf16[64,1024]{1,0:T(8,128)(2,1)S(1)}, bf16[64,1024]{1,0:T(8,128)(2,1)S(1)}, u32[]{:S(2)}, u32[]{:S(2)}) collective-permute-start(bf16[64,1024]{1,0:T(8,128)(2,1)S(1)} %pad_maximum_fusion.2), channel_id=1, source_target_pairs={{0,16},{8,24},{16,32},{24,40},{32,48},{40,56},{48,0},{56,8},{1,17}... | collective-permute-start | bytes 393224 | tf_op jit(solution)/shard_map/ppermute | solution.py:198
  41.4 29.5 %copy-start = (f32[1,1,2048]{2,1,0:T(1,128)S(1)}, f32[1,1,2048]{2,1,0:T(1,128)}, u32[]{:S(2)}) copy-start(f32[1,1,2048]{2,1,0:T(1,128)} %param.8) | copy-start | bytes 24580
  41.4 9.7 %collective-permute-start.2 = (bf16[128,1024]{1,0:T(8,128)(2,1)S(1)}, bf16[128,1024]{1,0:T(8,128)(2,1)S(1)}, u32[]{:S(2)}, u32[]{:S(2)}) collective-permute-start(bf16[128,1024]{1,0:T(8,128)(2,1)S(1)} %pad_maximum_fusion.1), channel_id=1, source_target_pairs={{0,8},{8,16},{16,24},{24,32},{32,40},{40,48},{48,56},{56,0},{1,9},... | collective-permute-start | bytes 786440 | tf_op jit(solution)/shard_map/ppermute | solution.py:198
  51.1 17.0 %collective-permute-start.3 = (bf16[256,1024]{1,0:T(8,128)(2,1)S(1)}, bf16[256,1024]{1,0:T(8,128)(2,1)S(1)}, u32[]{:S(2)}, u32[]{:S(2)}) collective-permute-start(bf16[256,1024]{1,0:T(8,128)(2,1)S(1)} %pad_maximum_fusion.refs_0_), channel_id=1, source_target_pairs={{0,2},{1,7},{2,4},{3,1},{4,6},{5,3},{6,0},{7,5},{8,10},{9,15},{10,... | collective-permute-start | bytes 1572872 | tf_op jit(solution)/shard_map/ppermute | solution.py:207
  54.5 37.7 %collective-permute-start.4 = (bf16[256,1024]{1,0:T(8,128)(2,1)S(1)}, bf16[256,1024]{1,0:T(8,128)(2,1)S(1)}, u32[]{:S(2)}, u32[]{:S(2)}) collective-permute-start(bf16[256,1024]{1,0:T(8,128)(2,1)S(1)} %pad_maximum_fusion.refs_0_), channel_id=1, source_target_pairs={{2,0},{7,1},{4,2},{1,3},{6,4},{3,5},{0,6},{5,7},{10,8},{15,9},{12,... | collective-permute-start | bytes 1572872 | tf_op jit(solution)/shard_map/ppermute | solution.py:207
  68.1 26.0 %collective-permute-start.5 = (bf16[256,1024]{1,0:T(8,128)(2,1)S(1)}, bf16[256,1024]{1,0:T(8,128)(2,1)S(1)}, u32[]{:S(2)}, u32[]{:S(2)}) collective-permute-start(bf16[256,1024]{1,0:T(8,128)(2,1)S(1)} %collective-permute-done.3.refs_1_), channel_id=1, source_target_pairs={{0,2},{1,7},{2,4},{3,1},{4,6},{5,3},{6,0},{7,5},{8,10},{9,15},{10,... | collective-permute-start | bytes 1572872 | tf_op jit(solution)/shard_map/ppermute | solution.py:208
  74.8 29.5 %all-to-all-start.1 = ((bf16[16,64,128]{2,1,0:T(8,128)(2,1)}), bf16[16,64,128]{2,1,0:T(8,128)(2,1)S(1)}, u32[]{:S(2)}, u32[]{:S(2)}) async-start(bf16[16,64,128]{2,1,0:T(8,128)(2,1)} %shard_map.56), calls=%async_computation.1 | async-start | bytes 524288 | tf_op jit(solution)/shard_map/all_to_all | solution.py:220
  87.8 8.8 %collective-permute-start.6 = (bf16[256,1024]{1,0:T(8,128)(2,1)S(1)}, bf16[256,1024]{1,0:T(8,128)(2,1)S(1)}, u32[]{:S(2)}, u32[]{:S(2)}) collective-permute-start(bf16[256,1024]{1,0:T(8,128)(2,1)S(1)} %pad_maximum_fusion.refs_0_), channel_id=1, source_target_pairs={{0,1},{1,0},{2,3},{3,2},{4,5},{5,4},{6,7},{7,6},{8,9},{9,8},{10,11... | collective-permute-start | bytes 1572872 | tf_op jit(solution)/shard_map/ppermute | solution.py:198
  89.8 6.9 %collective-permute-start.7 = (bf16[256,1024]{1,0:T(8,128)(2,1)S(1)}, bf16[256,1024]{1,0:T(8,128)(2,1)S(1)}, u32[]{:S(2)}, u32[]{:S(2)}) collective-permute-start(bf16[256,1024]{1,0:T(8,128)(2,1)S(1)} %collective-permute-done.3.refs_1_), channel_id=1, source_target_pairs={{0,1},{1,0},{2,3},{3,2},{4,5},{5,4},{6,7},{7,6},{8,9},{9,8},{10,11... | collective-permute-start | bytes 1572872 | tf_op jit(solution)/shard_map/ppermute | solution.py:198
  92.2 4.4 %collective-permute-start.8 = (bf16[256,1024]{1,0:T(8,128)(2,1)S(1)}, bf16[256,1024]{1,0:T(8,128)(2,1)}, u32[]{:S(2)}, u32[]{:S(2)}) collective-permute-start(bf16[256,1024]{1,0:T(8,128)(2,1)S(1)} %collective-permute-done.4.refs_2_), channel_id=1, source_target_pairs={{0,1},{1,0},{2,3},{3,2},{4,5},{5,4},{6,7},{7,6},{8,9},{9,8},{10,11... | collective-permute-start | bytes 1572872 | tf_op jit(solution)/shard_map/ppermute | solution.py:198
  94.1 4.1 %collective-permute-start.9 = (bf16[256,1024]{1,0:T(8,128)(2,1)S(1)}, bf16[256,1024]{1,0:T(8,128)(2,1)}, u32[]{:S(2)}, u32[]{:S(2)}) collective-permute-start(bf16[256,1024]{1,0:T(8,128)(2,1)S(1)} %collective-permute-done.5.refs_3_), channel_id=1, source_target_pairs={{0,1},{1,0},{2,3},{3,2},{4,5},{5,4},{6,7},{7,6},{8,9},{9,8},{10,11... | collective-permute-start | bytes 1572872 | tf_op jit(solution)/shard_map/ppermute | solution.py:198
